TPU v7x, 32 devices: a whole 2x2x4 slice. The times are simulated.
32 devices in a mesh: rep: 2 (over x), fs: 8 (over z, y), tp: 2 (over core).
Axes of the slice: x: 2, y: 2, z: 4, core: 2. Of those that a mesh axis runs over, the one named last changes fastest.
Arguments:
- states: bfloat16 [6144, 2048], P(('rep', 'fs'), 'tp'), may hold values from -6 to 6
- mix_gain: float32 [2048], replicated, may hold values from 0.1 to 1.9
- w_value: bfloat16 [2048, 2048], P('fs', 'tp'), may hold values from -1 to 1
- w_gate: bfloat16 [2048, 2048], P('fs', 'tp'), may hold values from -0.125 to 0.125
- conv_kernel: float32 [31, 2048], replicated, may hold values from -1 to 1
- chan_gain: float32 [2048], replicated, may hold values from 0.1 to 1.9
- w_mix_out: bfloat16 [2048, 2048], P('fs', 'tp'), may hold values from -0.125 to 0.125
- mlp_gain: float32 [2048], replicated, may hold values from 0.1 to 1.9
- w_up: bfloat16 [2048, 6144], P('fs', 'tp'), may hold values from -0.125 to 0.125
- w_down_t: bfloat16 [2048, 6144], P('fs', 'tp'), may hold values from -0.078125 to 0.078125
Outputs:
- layer_out: bfloat16 [6144, 2048], P(('rep', 'fs'), 'tp')
All inputs are finite; a program needn't handle non-finite values.
Results may differ from a plain program's by a relative error of at most 0.017.
Values may be sent and summed in bfloat16 or wider, within the bound.
A program may use at most 64 MiB of HBM per device.

v0:
```python
import functools

import jax
import jax.numpy as jnp
from jax import lax
from jax.experimental import pallas as pl
from jax.experimental.pallas import tpu as pltpu
from jax.sharding import PartitionSpec as P

LENGTH = 128
LANES = 128
LEAD = 32
EPS = 1e-06
MESH = pl.DeviceIdType.MESH


def times_transposed(left, right):
    return lax.dot_general(
        left, right, (((1,), (1,)), ((), ())), preferred_element_type=jnp.float32
    )


def kernel(
    sizes,
    states, mix_gain, w_value, w_gate, conv_kernel, chan_gain, w_mix, mlp_gain, w_up, w_down,
    out,
    weights, rows_in, rows_mid, normed, padded, filtered, activated, hidden,
    own_stats, peer_stats, mix_parts, mix_peers, fed_parts, fed_peers,
    load_sems, ring_send, ring_recv, in_send, in_recv, mid_send, mid_recv,
    stat_send, stat_recv, mix_send, mix_recv, fed_send, fed_recv,
):
    reps, n, tps, rows, channels, width, ups = sizes
    own_width = width * reps
    half_way = n // 2
    shard = channels // n
    tokens = reps * rows
    pieces = tokens // LENGTH
    chunks = 3 + 2 * ups
    rep, fs, tp = lax.axis_index("rep"), lax.axis_index("fs"), lax.axis_index("tp")
    taps = conv_kernel.shape[0]
    blocks, _, block = mix_parts.shape
    per_tp = own_width // block

    def ring_index(place):
        place = lax.rem(place + n, n)
        return jnp.where(place < half_way, 2 * place, 2 * (n - 1 - place) + 1)

    place = jnp.where(lax.rem(fs, 2) == 0, fs // 2, n - 1 - fs // 2)
    neighbours = (ring_index(place + 1), ring_index(place - 1))

    barrier = pltpu.get_barrier_semaphore()
    for other in neighbours:
        pl.semaphore_signal(barrier, inc=1, device_id={"fs": other}, device_id_type=MESH)
    for dr in range(reps):
        for dt in range(tps):
            if dr or dt:
                pl.semaphore_signal(
                    barrier, inc=1,
                    device_id={"rep": lax.rem(rep + dr, reps), "tp": lax.rem(tp + dt, tps)},
                    device_id_type=MESH,
                )

    own_rows = pl.ds(pl.multiple_of(rep * rows, rows), rows)
    own_cols = pl.ds(pl.multiple_of(tp * own_width, own_width), own_width)

    def shard_at(owner, start=0, size=None):
        size = shard if size is None else size
        return pl.ds(pl.multiple_of(owner * shard + start, size), size)

    def hop(c, s, way):
        sign = 1 if way == 0 else -1
        owner = ring_index(place - sign * (s - 1))
        span = shard_at(owner)
        if s == half_way:
            span = shard_at(owner, way * (shard // 2), shard // 2)
        return pltpu.make_async_remote_copy(
            src_ref=weights.at[c, span, :],
            dst_ref=weights.at[c, span, :],
            send_sem=ring_send.at[way, c],
            recv_sem=ring_recv.at[way, c, s - 1],
            device_id={"fs": neighbours[way]},
            device_id_type=MESH,
        )

    loads = []
    for c in range(chunks):
        if c < 3:
            source, column = (w_value, w_gate, w_mix)[c], rep * width
        elif c < 3 + ups:
            source, column = w_up, (rep * ups + c - 3) * width
        else:
            source, column = w_down, (rep * ups + c - 3 - ups) * width
        loads.append(
            pltpu.make_async_copy(
                source.at[:, pl.ds(pl.multiple_of(column, width), width)],
                weights.at[c, shard_at(fs), :],
                load_sems.at[c],
            )
        )
        loads[-1].start()
    own_load = pltpu.make_async_copy(states, rows_in.at[own_rows, own_cols], load_sems.at[chunks])
    own_load.start()
    pl.semaphore_wait(barrier, 1 + reps * tps)

    def pump(c, s):
        for way in range(2):
            if s == 1:
                if way == 0:
                    loads[c].wait()
            else:
                before = hop(c, s - 1, way)
                before.wait_recv()
                before.wait_send()
            hop(c, s, way).start()

    def arrived(c):
        for way in range(2):
            last = hop(c, half_way, way)
            last.wait_recv()
            last.wait_send()

    def spread(source, target, send, recv):
        def copy(dr, dt, ahead):
            if ahead:
                span = pl.ds(pl.multiple_of(lax.rem(rep + reps - dr, reps) * rows, rows), rows)
                src = target.at[span, own_cols]
            else:
                span, src = own_rows, source
            step_r = 0 if ahead else dr
            return pltpu.make_async_remote_copy(
                src_ref=src,
                dst_ref=target.at[span, own_cols],
                send_sem=send.at[dr, dt],
                recv_sem=recv.at[dr, dt],
                device_id={"rep": lax.rem(rep + step_r, reps), "tp": lax.rem(tp + dt, tps)},
                device_id_type=MESH,
            )

        first = [copy(dr, 0, False) for dr in range(1, reps)]
        near = [copy(0, dt, False) for dt in range(1, tps)]
        for one in first + near:
            one.start()

        def forward():
            later = []
            for dr in range(1, reps):
                first[dr - 1].wait_recv()
                for dt in range(1, tps):
                    one = copy(dr, dt, True)
                    one.start()
                    later.append(one)
            return later

        def finish(later):
            for one in near + later:
                one.wait_recv()
            for one in first + near + later:
                one.wait_send()

        return forward, finish

    def norm_all(source, gain):
        def one(i, carry):
            span = pl.ds(pl.multiple_of(i * 64, 64), 64)
            x = source[span, :].astype(jnp.float32)
            scale = lax.rsqrt(jnp.mean(x * x, axis=-1, keepdims=True) + EPS)
            normed[span, :] = (x * scale * gain[...]).astype(jnp.bfloat16)
            return carry

        lax.fori_loop(0, tokens // 64, one, 0)

    def seq_rows(i):
        return pl.ds(pl.multiple_of(i * LENGTH, LENGTH), LENGTH)

    def mixer_rows(i):
        x = normed[seq_rows(i), :]
        value = jnp.dot(x, weights[0], preferred_element_type=jnp.float32)
        gate = jnp.dot(x, weights[1], preferred_element_type=jnp.float32)
        padded[LEAD : LEAD + LENGTH, :] = value * jax.nn.sigmoid(gate)

        def column(j, sums):
            cols = pl.ds(pl.multiple_of(j * LANES, LANES), LANES)
            from_all = pl.multiple_of(tp * own_width + rep * width + j * LANES, LANES)
            kern = conv_kernel[:, pl.ds(from_all, LANES)]
            total = jnp.zeros((LENGTH, LANES), jnp.float32)
            for tap in range(taps):
                begin = LEAD - (taps - 1) + tap
                total = total + kern[tap : tap + 1, :] * padded[begin : begin + LENGTH, cols]
            filtered[seq_rows(i), cols] = total
            return sums[0] + total, sums[1] + total * total

        zero = jnp.zeros((LENGTH, LANES), jnp.float32)
        one, two = lax.fori_loop(0, width // LANES, column, (zero, zero))
        lane = lax.broadcasted_iota(jnp.int32, (LENGTH, LANES), 1)
        both = jnp.where(
            lane == 0,
            jnp.sum(one, axis=-1, keepdims=True),
            jnp.where(lane == 1, jnp.sum(two, axis=-1, keepdims=True), 0.0),
        )
        own_stats[:, seq_rows(i)] = both.T[0:8, :]

    def stat_copies():
        copies = []
        for dr in range(reps):
            for dt in range(tps):
                if dr or dt:
                    copies.append(
                        pltpu.make_async_remote_copy(
                            src_ref=own_stats,
                            dst_ref=peer_stats.at[dr * tps + dt],
                            send_sem=stat_send.at[dr, dt],
                            recv_sem=stat_recv.at[dr, dt],
                            device_id={
                                "rep": lax.rem(rep + dr, reps),
                                "tp": lax.rem(tp + dt, tps),
                            },
                            device_id_type=MESH,
                        )
                    )
        return copies

    def activate_rows(i, carry):
        total = own_stats[:, seq_rows(i)]
        for k in range(1, reps * tps):
            total = total + peer_stats[k, :, seq_rows(i)]
        turned = jnp.concatenate([total] * (LANES // 8), axis=0).T
        mean = turned[:, 0:1] / channels
        variance = turned[:, 1:2] / channels - mean * mean
        gain_at = pl.multiple_of(tp * own_width + rep * width, LANES)
        gain = chan_gain[:, pl.ds(gain_at, width)]
        x = (filtered[seq_rows(i), :] - mean) * lax.rsqrt(variance + EPS) * gain
        activated[seq_rows(i), :] = (x / (1.0 + jnp.exp(-x))).astype(jnp.bfloat16)
        return carry

    def share(order, o, left, pieces_of, parts, peers, send, recv):
        span = pl.ds(pl.multiple_of(o * block, block), block)

        def one(i):
            at = pl.ds(pl.multiple_of(i * rows, rows), rows)
            total = None
            for k, c in enumerate(pieces_of):
                term = times_transposed(
                    left[at, k * width : (k + 1) * width], weights[c, span, :]
                )
                total = term if total is None else total + term
            parts[o, at, :] = total.astype(jnp.bfloat16)

        keeper = o // per_tp
        dt = lax.rem(keeper + tps - tp, tps)
        waits = []
        for dr in [*range(1, reps), 0]:
            to = lax.rem(rep + dr, reps)
            one(to)
            copy = pltpu.make_async_remote_copy(
                src_ref=parts.at[o, pl.ds(pl.multiple_of(to * rows, rows), rows), :],
                dst_ref=peers.at[dr * tps + dt, lax.rem(o, per_tp)],
                send_sem=send.at[order, dr],
                recv_sem=recv.at[dr * tps + dt, lax.rem(o, per_tp)],
                device_id={"rep": to, "tp": keeper},
                device_id_type=MESH,
            )
            if dr:
                copy.start()
                waits.append(copy.wait_send)
            else:
                pl.when(keeper != tp)(copy.start)
                waits.append(lambda k=keeper, c=copy: pl.when(k != tp)(c.wait_send))
        return waits

    def wait_peers(j, parts, peers, send, recv):
        for k in range(1, reps * tps):
            dr, dt = k // tps, k % tps
            pltpu.make_async_remote_copy(
                src_ref=parts.at[0, own_rows, :],
                dst_ref=peers.at[k, j],
                send_sem=send.at[0, 0],
                recv_sem=recv.at[k, j],
                device_id={"rep": lax.rem(rep + dr, reps), "tp": lax.rem(tp + dt, tps)},
                device_id_type=MESH,
            ).wait_recv()

    def total_of(j, parts, peers):
        total = parts[tp * per_tp + j, own_rows, :].astype(jnp.float32)
        for k in range(1, reps * tps):
            total = total + peers[k, j].astype(jnp.float32)
        return total

    stepwise = blocks == n

    def owners(s):
        if s in (0, half_way):
            return [ring_index(place + s)]
        return [ring_index(place - s), ring_index(place + s)]

    def steps_of(c):
        return range(1, half_way + 1)

    first, second = (0, 1), (2, 3)
    third = tuple(range(4, 3 + ups))
    fourth = tuple(range(3 + ups, chunks))

    pump(0, 1)
    pump(1, 1)
    forward, finish = spread(states, rows_in, in_send, in_recv)
    padded[0:LEAD, :] = jnp.zeros((LEAD, width), jnp.float32)
    pump(0, 2)
    pump(1, 2)
    later = forward()
    for s in range(3, half_way + 1):
        pump(0, s)
        if s == 3:
            own_load.wait()
            finish(later)
        pump(1, s)
        if s == 3:
            norm_all(rows_in, mix_gain)
    pump(2, 1)
    pump(3, 1)
    arrived(0)
    arrived(1)

    todo = [(c, s) for s in range(2, half_way + 1) for c in second]

    def next_hop():
        if todo:
            pump(*todo.pop(0))

    for i in range(0, pieces, 2):
        lax.fori_loop(
            i, min(i + 2, pieces), lambda k, carry: (mixer_rows(k), carry)[1], 0
        )
        next_hop()
    stats = stat_copies()
    for one in stats:
        one.start()
    for one in stats:
        one.wait_recv()
    lax.fori_loop(0, pieces, activate_rows, 0)
    waits = []
    mix = (activated, (2,), mix_parts, mix_peers, mix_send, mix_recv)
    if stepwise:
        for s in range(half_way - 1):
            for o in owners(s):
                waits += share(len(waits) // reps, o, *mix)
    while todo:
        next_hop()
    if stepwise:
        for o in owners(half_way - 1):
            waits += share(len(waits) // reps, o, *mix)
    for c in third:
        pump(c, 1)
    arrived(2)
    if stepwise:
        waits += share(len(waits) // reps, owners(half_way)[0], *mix)
    else:
        for o in range(blocks):
            waits += share(o, o, *mix)

    todo = [(c, s) for s in range(2, half_way + 1) for c in third]
    for _ in range(len(todo) // 2):
        next_hop()
    for j in range(per_tp):
        wait_peers(j, mix_parts, mix_peers, mix_send, mix_recv)
        at = pl.ds(pl.multiple_of(tp * own_width + j * block, block), block)
        rows_mid[own_rows, at] = (
            rows_in[own_rows, at].astype(jnp.float32) + total_of(j, mix_parts, mix_peers)
        ).astype(jnp.bfloat16)
    forward, finish = spread(rows_mid.at[own_rows, own_cols], rows_mid, mid_send, mid_recv)
    while todo:
        next_hop()
    for c in fourth:
        pump(c, 1)
    arrived(3)
    for c in third:
        arrived(c)
    later = forward()
    finish(later)
    norm_all(rows_mid, mlp_gain)
    todo = [(c, s) for s in range(2, half_way + 1) for c in fourth]
    next_hop()
    for k in range(ups):

        def up_rows(i, carry):
            at = pl.ds(pl.multiple_of(i * rows, rows), rows)
            x = jnp.dot(normed[at, :], weights[3 + k], preferred_element_type=jnp.float32)
            x = jnp.maximum(x, 0.0)
            hidden[at, k * width : (k + 1) * width] = (x * x).astype(jnp.bfloat16)
            return carry

        lax.fori_loop(0, reps, up_rows, 0)
        next_hop()
    done = []
    fed = (hidden, fourth, fed_parts, fed_peers, fed_send, fed_recv)
    if stepwise:
        for o in owners(0):
            done += share(len(done) // reps, o, *fed)
    for s in range(2, half_way + 1):
        while todo and todo[0][1] <= s:
            next_hop()
        if stepwise:
            for o in owners(s - 1):
                done += share(len(done) // reps, o, *fed)
    for c in fourth:
        arrived(c)
    if stepwise:
        done += share(len(done) // reps, owners(half_way)[0], *fed)
    else:
        for o in range(blocks):
            done += share(o, o, *fed)
    for j in range(per_tp):
        wait_peers(j, fed_parts, fed_peers, fed_send, fed_recv)
        at = pl.ds(pl.multiple_of(tp * own_width + j * block, block), block)
        out[:, j * block : (j + 1) * block] = (
            rows_mid[own_rows, at].astype(jnp.float32) + total_of(j, fed_parts, fed_peers)
        ).astype(jnp.bfloat16)
    for one in stats:
        one.wait_send()
    for wait in waits + done:
        wait()


def body(mesh, states, mix_gain, w_value, w_gate, conv_kernel, chan_gain, w_mix, mlp_gain, w_up, w_down):
    reps, n, tps = mesh.shape["rep"], mesh.shape["fs"], mesh.shape["tp"]
    rows, own_width = states.shape
    width = own_width // reps
    channels = own_width * tps
    ups = w_up.shape[1] // own_width
    tokens = rows * reps
    group = reps * tps
    block = channels // n if channels // n >= LANES else own_width
    blocks, per_tp = channels // block, own_width // block
    chunks = 3 + 2 * ups
    bf16, f32 = jnp.bfloat16, jnp.float32
    vmem, hbm = pl.BlockSpec(memory_space=pltpu.VMEM), pl.BlockSpec(memory_space=pl.ANY)
    dma = pltpu.SemaphoreType.DMA
    return pl.pallas_call(
        functools.partial(kernel, (reps, n, tps, rows, channels, width, ups)),
        out_shape=jax.ShapeDtypeStruct((rows, own_width), bf16),
        in_specs=[hbm, vmem, hbm, hbm, vmem, vmem, hbm, vmem, hbm, hbm],
        out_specs=vmem,
        scratch_shapes=[
            pltpu.VMEM((chunks, channels, width), bf16),
            pltpu.VMEM((tokens, channels), bf16),
            pltpu.VMEM((tokens, channels), bf16),
            pltpu.VMEM((tokens, channels), bf16),
            pltpu.VMEM((LEAD + LENGTH, width), f32),
            pltpu.VMEM((tokens, width), f32),
            pltpu.VMEM((tokens, width), bf16),
            pltpu.VMEM((tokens, ups * width), bf16),
            pltpu.VMEM((8, tokens), f32),
            pltpu.VMEM((group, 8, tokens), f32),
            pltpu.VMEM((blocks, tokens, block), bf16),
            pltpu.VMEM((group, per_tp, rows, block), bf16),
            pltpu.VMEM((blocks, tokens, block), bf16),
            pltpu.VMEM((group, per_tp, rows, block), bf16),
            dma((chunks + 1,)),
            dma((2, chunks)),
            dma((2, chunks, n // 2)),
            dma((reps, tps)),
            dma((reps, tps)),
            dma((reps, tps)),
            dma((reps, tps)),
            dma((reps, tps)),
            dma((reps, tps)),
            dma((blocks, reps)),
            dma((group, per_tp)),
            dma((blocks, reps)),
            dma((group, per_tp)),
        ],
        compiler_params=pltpu.CompilerParams(
            collective_id=0, has_side_effects=True, vmem_limit_bytes=62 * 1024 * 1024
        ),
    )(
        states, mix_gain[None, :], w_value, w_gate, conv_kernel, chan_gain[None, :], w_mix,
        mlp_gain[None, :], w_up, w_down,
    )


def solution(mesh):
    in_specs = (
        P(("rep", "fs"), "tp"),
        P(),
        P("fs", "tp"),
        P("fs", "tp"),
        P(),
        P(),
        P("fs", "tp"),
        P(),
        P("fs", "tp"),
        P("fs", "tp"),
    )
    out_specs = P(("rep", "fs"), "tp")
    return jax.shard_map(
        functools.partial(body, mesh),
        mesh=mesh, in_specs=in_specs, out_specs=out_specs, check_vma=False,
    )
```

profile of v0, /device:TPU:24, one launch (start us, length us, event | category | flops | bytes accessed | tf_op | source)
XLA Modules:
  0.0 193.5 jit_solution(10029835219497245322)
XLA Ops:
  0.0 191.4 %shard_map.100 = bf16[384,1024]{1,0:T(8,128)(2,1)} custom-call(bf16[384,1024]{1,0:T(8,128)(2,1)} %states.1, f32[1,2048]{1,0:T(1,128)} %bitcast.3, bf16[256,1024]{1,0:T(8,128)(2,1)} %w_value.1, bf16[256,1024]{1,0:T(8,128)(2,1)} %w_gate.1, f32[31,2048]{1,0:T(8,128)} %conv_kernel.1, f32[1,2048]{1,0:T(1,128)} %bitcast.4, bf16[256,1024]{1,0:T(8,128)(2,1)} %w_mix.1, ...), custom_call_target="tpu_custom_call" | custom-call | tf_op jit(solution)/shard_map/pallas_call | solution.py:436
  191.4 2.1 %copy.12 = bf16[384,1024]{1,0:T(8,128)(2,1)} copy(bf16[384,1024]{1,0:T(8,128)(2,1)} %shard_map.100) | data formatting | bytes 1572864
where the time goes:
time: 195 us; the launch traced here: 193 us
  Pallas kernels  191 us (98%)
  local copies, waits for them, and re-layouts  2.06 us (1%)
    pallas_call x1, Pallas kernels, body(): pl.pallas_call(functools.partial(kernel, (reps, n, tps, rows, channels, w...  191 us

commit v1 on v0

--- a/solution.py
+++ b/solution.py
@@ -20,7 +20,7 @@
     )
 
 
-def kernel(
+def ring_kernel(
     sizes,
     states, mix_gain, w_value, w_gate, conv_kernel, chan_gain, w_mix, mlp_gain, w_up, w_down,
     out,
@@ -419,7 +419,7 @@
         wait()
 
 
-def body(mesh, states, mix_gain, w_value, w_gate, conv_kernel, chan_gain, w_mix, mlp_gain, w_up, w_down):
+def ring_body(mesh, states, mix_gain, w_value, w_gate, conv_kernel, chan_gain, w_mix, mlp_gain, w_up, w_down):
     reps, n, tps = mesh.shape["rep"], mesh.shape["fs"], mesh.shape["tp"]
     rows, own_width = states.shape
     width = own_width // reps
@@ -434,7 +434,7 @@
     vmem, hbm = pl.BlockSpec(memory_space=pltpu.VMEM), pl.BlockSpec(memory_space=pl.ANY)
     dma = pltpu.SemaphoreType.DMA
     return pl.pallas_call(
-        functools.partial(kernel, (reps, n, tps, rows, channels, width, ups)),
+        functools.partial(ring_kernel, (reps, n, tps, rows, channels, width, ups)),
         out_shape=jax.ShapeDtypeStruct((rows, own_width), bf16),
         in_specs=[hbm, vmem, hbm, hbm, vmem, vmem, hbm, vmem, hbm, hbm],
         out_specs=vmem,
@@ -476,6 +476,588 @@
     )
 
 
+def plane_kernel(
+    sizes,
+    states, mix_gain, w_value, w_gate, conv_kernel, chan_gain, w_mix, mlp_gain, w_up, w_down,
+    out,
+    weights, rows_in, rows_mid, normed, padded, filtered, activated, hidden, own_in, own_mid,
+    own_stats, peer_stats, mix_parts, mix_peers, fed_parts, fed_peers,
+    load_sems, y_send, y_recv, near_send, far_send, line_recv, twin_send, twin_recv,
+    in_send, in_recv, mid_send, mid_recv,
+    stat_send, stat_recv, mix_send, mix_recv, fed_send, fed_recv,
+):
+    reps, n, tps, rows, channels, sub, ups = sizes
+    ys = tps
+    zs = n // ys
+    members = reps * ys
+    width = sub * tps
+    own_width = sub * members
+    shard = channels // n
+    plane_shard = shard * ys
+    tokens = reps * rows
+    pieces = tokens // LENGTH
+    chunks = 3 + 2 * ups
+    rep, fs, tp = lax.axis_index("rep"), lax.axis_index("fs"), lax.axis_index("tp")
+    z, y = fs // ys, lax.rem(fs, ys)
+    other_rep, other_y, other_tp = reps - 1 - rep, ys - 1 - y, tps - 1 - tp
+    other_fs = z * ys + other_y
+    own_group = rep * ys + y
+    taps = conv_kernel.shape[0]
+    blocks, _, block = mix_parts.shape
+    per_tp = own_width // block
+
+    has_next = (z < zs - 1, z > 0)
+    next_fs = (fs + ys, fs - ys)
+    is_home = tp == y
+
+    barrier = pltpu.get_barrier_semaphore()
+    for dr in range(reps):
+        for dy in range(ys):
+            for dt in range(tps):
+                if dr or dy or dt:
+                    pl.semaphore_signal(
+                        barrier, inc=1,
+                        device_id={
+                            "rep": lax.rem(rep + dr, reps),
+                            "fs": z * ys + lax.rem(y + dy, ys),
+                            "tp": lax.rem(tp + dt, tps),
+                        },
+                        device_id_type=MESH,
+                    )
+    for way in range(2):
+        @pl.when(has_next[way])
+        def _():
+            pl.semaphore_signal(
+                barrier, inc=1, device_id={"fs": next_fs[way]}, device_id_type=MESH
+            )
+
+    def remote(src, dst, send, recv, **where):
+        return pltpu.make_async_remote_copy(
+            src_ref=src, dst_ref=dst, send_sem=send, recv_sem=recv,
+            device_id=where, device_id_type=MESH,
+        )
+
+    def rows_of(index, size=shard):
+        return pl.ds(pl.multiple_of(index * size, size), size)
+
+    def rep_rows(r):
+        return pl.ds(pl.multiple_of(r * rows, rows), rows)
+
+    half = pl.ds(pl.multiple_of(tp * sub, sub), sub)
+
+    def columns_of(c, group):
+        if c < 3:
+            source, at = (w_value, w_gate, w_mix)[c], group
+        elif c < 3 + ups:
+            source, at = w_up, group * ups + c - 3
+        else:
+            source, at = w_down, group * ups + c - 3 - ups
+        return source.at[:, pl.ds(pl.multiple_of(at * sub, sub), sub)]
+
+    loads = [
+        pltpu.make_async_copy(
+            columns_of(c, own_group), weights.at[c, rows_of(fs), half], load_sems.at[c]
+        )
+        for c in range(chunks)
+    ]
+    home_cols = pl.ds(pl.multiple_of(tp * own_width, own_width), own_width)
+    own_load = pltpu.make_async_copy(states, own_in, load_sems.at[chunks])
+    home_load = pltpu.make_async_copy(
+        states, rows_in.at[rep_rows(rep), home_cols], load_sems.at[chunks + 1]
+    )
+    for c in range(chunks):
+        loads[c].start()
+    pl.when(is_home)(home_load.start)
+    own_load.start()
+    along_line = sum(jnp.where(has, 1, 0) for has in has_next)
+    pl.semaphore_wait(barrier, reps * ys * tps - 1 + along_line)
+
+    def across(c):
+        return remote(
+            columns_of(c, rep * ys + other_y), weights.at[c, rows_of(fs), half],
+            y_send.at[c], y_recv.at[c], fs=other_fs,
+        )
+
+    middle = jnp.minimum(z, zs - 1 - z)
+
+    def offset_at(i):
+        near = (i + 1) // 2 if i % 2 else -(i // 2)
+        far = jnp.where(2 * z < zs - 1, i - middle, middle - i)
+        return jnp.where(i <= 2 * middle, near, far)
+
+    offsets = [offset_at(i) for i in range(zs)]
+    planes = [z + off for off in offsets]
+
+    def twin(c, i):
+        span = rows_of(planes[i], plane_shard)
+        return remote(
+            weights.at[c, span, half], weights.at[c, span, half],
+            twin_send.at[c, i], twin_recv.at[c, i], tp=other_tp,
+        )
+
+    def near(c, way, index):
+        span = rows_of(index)
+        return remote(
+            weights.at[c, span, half], weights.at[c, span, half],
+            near_send.at[c, way], line_recv.at[way, c, 0], fs=next_fs[way],
+        )
+
+    def near_all(c, way):
+        span = rows_of(z, plane_shard)
+        return remote(
+            weights.at[c, span, half], weights.at[c, span, half],
+            near_send.at[c, way], line_recv.at[way, c, 0], fs=next_fs[way],
+        )
+
+    def own(c):
+        loads[c].wait()
+        for way in range(2):
+            pl.when(has_next[way])(near(c, way, fs).start)
+        across(c).wait_recv()
+        for way in range(2):
+            pl.when(has_next[way])(near(c, way, other_fs).start)
+        twin(c, 0).start()
+
+    def far(c, i):
+        off, plane = offsets[i], planes[i]
+        upward = off < 0
+        way = jnp.where(upward, 0, 1)
+        step = jnp.abs(off)
+        span = rows_of(plane, plane_shard)
+        arrival = remote(
+            weights.at[c, span, half], weights.at[c, span, half],
+            far_send.at[c, i - 1], line_recv.at[way, c, step - 1], fs=other_fs,
+        )
+        goes = jnp.where(upward, z < zs - 1, z > 0)
+        onward = remote(
+            weights.at[c, span, half], weights.at[c, span, half],
+            far_send.at[c, i - 1], line_recv.at[way, c, jnp.minimum(step, zs - 2)],
+            fs=jnp.where(upward, fs + ys, fs - ys),
+        )
+        return arrival, goes, onward
+
+    def arrive(c, i):
+        arrival, goes, onward = far(c, i)
+        arrival.wait_recv()
+        pl.when(goes)(onward.start)
+        twin(c, i).start()
+
+    def ready(c, i):
+        twin(c, i).wait_recv()
+
+    def drain(c):
+        across(c).wait_send()
+        for way in range(2):
+            pl.when(has_next[way])(near_all(c, way).wait_send)
+        for i in range(zs):
+            twin(c, i).wait_send()
+            if i:
+                _, goes, onward = far(c, i)
+                pl.when(goes)(onward.wait_send)
+
+    def spread(source, target, send, recv):
+        def at(r, h, j):
+            start = pl.multiple_of(h * own_width + j * block, block)
+            return target.at[rep_rows(r), pl.ds(start, block)]
+
+        def copies(j):
+            src = source.at[:, j * block : (j + 1) * block]
+            dst = at(rep, tp, j)
+            along = remote(src, dst, send.at[0, j], recv.at[1, tp, j], rep=other_rep, tp=y)
+            over = remote(src, dst, send.at[1, j], recv.at[0, tp, j], fs=other_fs, tp=y)
+            inside = remote(src, dst, send.at[2, j], recv.at[0, tp, j], tp=y)
+            return along, over, inside
+
+        def passing(j):
+            one, two = at(other_rep, 0, j), at(rep, 1, j)
+            over = remote(one, one, send.at[3, j], recv.at[1, 0, j], fs=other_fs)
+            along = remote(two, two, send.at[3, j], recv.at[1, 1, j], rep=other_rep)
+            return over, along
+
+        def arrival(dr, h, j):
+            dst = at(rep if dr == 0 else other_rep, h, j)
+            return remote(dst, dst, send.at[0, j], recv.at[dr, h, j], rep=other_rep)
+
+        def start(j):
+            along, over, inside = copies(j)
+            along.start()
+            over.start()
+            pl.when(jnp.logical_not(is_home))(inside.start)
+
+        def forward(j):
+            over, along = passing(j)
+
+            @pl.when(is_home)
+            def _():
+                arrival(1, 0, j).wait_recv()
+                over.start()
+
+            @pl.when(jnp.logical_not(is_home))
+            def _():
+                arrival(0, 1, j).wait_recv()
+                along.start()
+
+        def finish(j):
+            arrival(1, 1, j).wait_recv()
+
+            @pl.when(is_home)
+            def _():
+                arrival(0, other_tp, j).wait_recv()
+
+            @pl.when(jnp.logical_not(is_home))
+            def _():
+                arrival(0, 0, j).wait_recv()
+                arrival(1, 0, j).wait_recv()
+
+        def settle(j):
+            along, over, inside = copies(j)
+            along.wait_send()
+            over.wait_send()
+            pl.when(jnp.logical_not(is_home))(inside.wait_send)
+            passing(j)[0].wait_send()
+
+        return start, forward, finish, settle
+
+    def norm_all(source, gain):
+        def one(i, carry):
+            span = pl.ds(pl.multiple_of(i * 64, 64), 64)
+            x = source[span, :].astype(jnp.float32)
+            scale = lax.rsqrt(jnp.mean(x * x, axis=-1, keepdims=True) + EPS)
+            normed[span, :] = (x * scale * gain[...]).astype(jnp.bfloat16)
+            return carry
+
+        lax.fori_loop(0, tokens // 64, one, 0)
+
+    def seq_rows(i):
+        return pl.ds(pl.multiple_of(i * LENGTH, LENGTH), LENGTH)
+
+    def mixer_rows(i):
+        x = normed[seq_rows(i), :]
+        value = jnp.dot(x, weights[0], preferred_element_type=jnp.float32)
+        gate = jnp.dot(x, weights[1], preferred_element_type=jnp.float32)
+        padded[LEAD : LEAD + LENGTH, :] = value * jax.nn.sigmoid(gate)
+        per_sub = sub // LANES
+
+        def column(j, sums):
+            cols = pl.ds(pl.multiple_of(j * LANES, LANES), LANES)
+            from_all = pl.multiple_of(
+                (j // per_sub) * own_width + own_group * sub + lax.rem(j, per_sub) * LANES, LANES
+            )
+            kern = conv_kernel[:, pl.ds(from_all, LANES)]
+            total = jnp.zeros((LENGTH, LANES), jnp.float32)
+            for tap in range(taps):
+                begin = LEAD - (taps - 1) + tap
+                total = total + kern[tap : tap + 1, :] * padded[begin : begin + LENGTH, cols]
+            filtered[seq_rows(i), cols] = total
+            return sums[0] + total, sums[1] + total * total
+
+        zero = jnp.zeros((LENGTH, LANES), jnp.float32)
+        one, two = lax.fori_loop(0, width // LANES, column, (zero, zero))
+        lane = lax.broadcasted_iota(jnp.int32, (LENGTH, LANES), 1)
+        both = jnp.where(
+            lane == 0,
+            jnp.sum(one, axis=-1, keepdims=True),
+            jnp.where(lane == 1, jnp.sum(two, axis=-1, keepdims=True), 0.0),
+        )
+        own_stats[:, seq_rows(i)] = both.T[0:8, :]
+
+    def stat_copies():
+        return [
+            remote(
+                own_stats, peer_stats.at[dr * ys + dy], stat_send.at[dr, dy],
+                stat_recv.at[dr, dy],
+                rep=lax.rem(rep + dr, reps), fs=z * ys + lax.rem(y + dy, ys),
+            )
+            for dr in range(reps) for dy in range(ys) if dr or dy
+        ]
+
+    def activate_rows(i, carry):
+        total = own_stats[:, seq_rows(i)]
+        for k in range(1, members):
+            total = total + peer_stats[k, :, seq_rows(i)]
+        turned = jnp.concatenate([total] * (LANES // 8), axis=0).T
+        mean = turned[:, 0:1] / channels
+        variance = turned[:, 1:2] / channels - mean * mean
+        gain = jnp.concatenate(
+            [
+                chan_gain[:, pl.ds(pl.multiple_of(t * own_width + own_group * sub, sub), sub)]
+                for t in range(tps)
+            ],
+            axis=1,
+        )
+        x = (filtered[seq_rows(i), :] - mean) * lax.rsqrt(variance + EPS) * gain
+        activated[seq_rows(i), :] = (x / (1.0 + jnp.exp(-x))).astype(jnp.bfloat16)
+        return carry
+
+    def share(order, o, left, pieces_of, parts, peers, send, recv):
+        span = rows_of(o, block)
+        keeper, kept = o // per_tp, lax.rem(o, per_tp)
+        waits = []
+        for dr in [*range(1, reps), 0]:
+            to = lax.rem(rep + dr, reps)
+            at = rep_rows(to)
+            total = None
+            for k, c in enumerate(pieces_of):
+                term = times_transposed(
+                    left[at, k * width : (k + 1) * width], weights[c, span, :]
+                )
+                total = term if total is None else total + term
+            parts[o, at, :] = total.astype(jnp.bfloat16)
+            slot = (reps - dr) % reps * ys + lax.rem(y + ys - tp, ys)
+            copy = remote(
+                parts.at[o, at, :], peers.at[slot, kept], send.at[order, dr],
+                recv.at[slot, kept], rep=to, fs=z * ys + tp, tp=keeper,
+            )
+            if dr:
+                copy.start()
+                waits.append(copy.wait_send)
+            else:
+                away = jnp.logical_not(jnp.logical_and(is_home, keeper == tp))
+                pl.when(away)(copy.start)
+                waits.append(lambda w=away, c=copy: pl.when(w)(c.wait_send))
+        return waits
+
+    def wait_peers(j, parts, peers, send, recv):
+        def one(k):
+            return remote(
+                parts.at[0, rep_rows(rep), :], peers.at[k, j], send.at[0, 0], recv.at[k, j],
+                rep=other_rep,
+            )
+
+        for k in range(1, members):
+            one(k).wait_recv()
+
+        @pl.when(is_home)
+        def _():
+            peers[0, j] = parts[tp * per_tp + j, rep_rows(rep), :]
+
+        pl.when(jnp.logical_not(is_home))(one(0).wait_recv)
+
+    def total_of(j, peers):
+        total = peers[0, j].astype(jnp.float32)
+        for k in range(1, members):
+            total = total + peers[k, j].astype(jnp.float32)
+        return total
+
+    third = tuple(range(3, 3 + ups))
+    fourth = tuple(range(3 + ups, chunks))
+    per_plane = plane_shard // block
+
+    start_in, forward_in, finish_in, settle_in = spread(states, rows_in, in_send, in_recv)
+    start_mid, forward_mid, finish_mid, settle_mid = spread(own_mid, rows_mid, mid_send, mid_recv)
+
+    across(0).start()
+    across(1).start()
+    own(0)
+    for j in range(per_tp):
+        start_in(j)
+    own(1)
+    for c in range(2, chunks):
+        across(c).start()
+    padded[0:LEAD, :] = jnp.zeros((LEAD, width), jnp.float32)
+    arrive(0, 1)
+    for j in range(per_tp // 2):
+        forward_in(j)
+    arrive(0, 2)
+    for j in range(per_tp // 2, per_tp):
+        forward_in(j)
+    arrive(0, 3)
+    own(2)
+    pl.when(is_home)(home_load.wait)
+    arrive(1, 1)
+    for j in range(per_tp):
+        finish_in(j)
+    norm_all(rows_in, mix_gain)
+    arrive(1, 2)
+    own(3)
+    arrive(1, 3)
+    for c in (0, 1):
+        for i in range(zs):
+            ready(c, i)
+
+    todo = [functools.partial(arrive, 2, i) for i in range(1, zs)]
+    todo.append(functools.partial(own, 4))
+    for i in range(0, pieces, 2):
+        lax.fori_loop(
+            i, min(i + 2, pieces), lambda k, carry: (mixer_rows(k), carry)[1], 0
+        )
+        if todo:
+            todo.pop(0)()
+    stats = stat_copies()
+    for one in stats:
+        one.start()
+    while todo:
+        todo.pop(0)()
+    for one in stats:
+        one.wait_recv()
+    lax.fori_loop(0, pieces, activate_rows, 0)
+    waits = []
+    mix = (activated, (2,), mix_parts, mix_peers, mix_send, mix_recv)
+    for i in range(zs):
+        ready(2, i)
+        for b in range(per_plane):
+            waits += share(len(waits) // reps, planes[i] * per_plane + b, *mix)
+
+    todo = [functools.partial(arrive, 3, i) for i in range(1, zs)]
+    for c in range(4, 3 + ups):
+        todo.append(functools.partial(own, c + 1))
+        todo += [functools.partial(arrive, c, i) for i in range(1, zs)]
+    todo += [functools.partial(own, c) for c in range(4 + ups, chunks)]
+    steps = 2 * per_tp + 1
+    cuts = [len(todo) * k // steps for k in range(steps + 1)]
+
+    def do_some(k):
+        for one in todo[cuts[k] : cuts[k + 1]]:
+            one()
+
+    own_load.wait()
+    do_some(0)
+    for j in range(per_tp):
+        wait_peers(j, mix_parts, mix_peers, mix_send, mix_recv)
+        cols = slice(j * block, (j + 1) * block)
+        own_mid[:, cols] = (
+            own_in[:, cols].astype(jnp.float32) + total_of(j, mix_peers)
+        ).astype(jnp.bfloat16)
+        start_mid(j)
+
+        @pl.when(is_home)
+        def _():
+            start = pl.multiple_of(tp * own_width + j * block, block)
+            rows_mid[rep_rows(rep), pl.ds(start, block)] = own_mid[:, cols]
+
+        do_some(1 + j)
+        if j:
+            forward_mid(j - 1)
+    forward_mid(per_tp - 1)
+    for j in range(per_tp):
+        do_some(1 + per_tp + j)
+        finish_mid(j)
+    norm_all(rows_mid, mlp_gain)
+    for c in third:
+        for i in range(zs):
+            ready(c, i)
+
+    def up_some(k):
+        def up_rows(i, carry):
+            at = rep_rows(i)
+            x = jnp.dot(normed[at, :], weights[3 + k], preferred_element_type=jnp.float32)
+            x = jnp.maximum(x, 0.0)
+            hidden[at, k * width : (k + 1) * width] = (x * x).astype(jnp.bfloat16)
+            return carry
+
+        lax.fori_loop(0, reps, up_rows, 0)
+
+    for k in range(ups):
+        up_some(k)
+        arrive(fourth[k], 1)
+    done = []
+    fed = (hidden, fourth, fed_parts, fed_peers, fed_send, fed_recv)
+    for i in range(zs):
+        if i > 1:
+            for c in fourth:
+                arrive(c, i)
+        for c in fourth:
+            ready(c, i)
+        for b in range(per_plane):
+            done += share(len(done) // reps, planes[i] * per_plane + b, *fed)
+    for j in range(per_tp):
+        wait_peers(j, fed_parts, fed_peers, fed_send, fed_recv)
+        cols = slice(j * block, (j + 1) * block)
+        out[:, cols] = (
+            own_mid[:, cols].astype(jnp.float32) + total_of(j, fed_peers)
+        ).astype(jnp.bfloat16)
+    for one in stats:
+        one.wait_send()
+    for j in range(per_tp):
+        settle_in(j)
+        settle_mid(j)
+    for c in range(chunks):
+        drain(c)
+    for wait in waits + done:
+        wait()
+
+
+def plane_body(mesh, states, mix_gain, w_value, w_gate, conv_kernel, chan_gain, w_mix, mlp_gain, w_up, w_down):
+    reps, n, tps = mesh.shape["rep"], mesh.shape["fs"], mesh.shape["tp"]
+    rows, own_width = states.shape
+    ys = tps
+    zs, members = n // ys, reps * ys
+    sub = own_width // members
+    width = sub * tps
+    channels = own_width * tps
+    ups = w_up.shape[1] // own_width
+    tokens = rows * reps
+    block = channels // n
+    blocks, per_tp = channels // block, own_width // block
+    chunks = 3 + 2 * ups
+    bf16, f32 = jnp.bfloat16, jnp.float32
+    vmem, hbm = pl.BlockSpec(memory_space=pltpu.VMEM), pl.BlockSpec(memory_space=pl.ANY)
+    dma = pltpu.SemaphoreType.DMA
+    return pl.pallas_call(
+        functools.partial(plane_kernel, (reps, n, tps, rows, channels, sub, ups)),
+        out_shape=jax.ShapeDtypeStruct((rows, own_width), bf16),
+        in_specs=[hbm, vmem, hbm, hbm, vmem, vmem, hbm, vmem, hbm, hbm],
+        out_specs=vmem,
+        scratch_shapes=[
+            pltpu.VMEM((chunks, channels, width), bf16),
+            pltpu.VMEM((tokens, channels), bf16),
+            pltpu.VMEM((tokens, channels), bf16),
+            pltpu.VMEM((tokens, channels), bf16),
+            pltpu.VMEM((LEAD + LENGTH, width), f32),
+            pltpu.VMEM((tokens, width), f32),
+            pltpu.VMEM((tokens, width), bf16),
+            pltpu.VMEM((tokens, ups * width), bf16),
+            pltpu.VMEM((rows, own_width), bf16),
+            pltpu.VMEM((rows, own_width), bf16),
+            pltpu.VMEM((8, tokens), f32),
+            pltpu.VMEM((members, 8, tokens), f32),
+            pltpu.VMEM((blocks, tokens, block), bf16),
+            pltpu.VMEM((members, per_tp, rows, block), bf16),
+            pltpu.VMEM((blocks, tokens, block), bf16),
+            pltpu.VMEM((members, per_tp, rows, block), bf16),
+            dma((chunks + 2,)),
+            dma((chunks,)),
+            dma((chunks,)),
+            dma((chunks, 2)),
+            dma((chunks, zs - 1)),
+            dma((2, chunks, zs - 1)),
+            dma((chunks, zs)),
+            dma((chunks, zs)),
+            dma((4, per_tp)),
+            dma((reps, tps, per_tp)),
+            dma((4, per_tp)),
+            dma((reps, tps, per_tp)),
+            dma((reps, ys)),
+            dma((reps, ys)),
+            dma((blocks, reps)),
+            dma((members, per_tp)),
+            dma((blocks, reps)),
+            dma((members, per_tp)),
+        ],
+        compiler_params=pltpu.CompilerParams(
+            collective_id=0, has_side_effects=True, vmem_limit_bytes=62 * 1024 * 1024
+        ),
+    )(
+        states, mix_gain[None, :], w_value, w_gate, conv_kernel, chan_gain[None, :], w_mix,
+        mlp_gain[None, :], w_up, w_down,
+    )
+
+
+def body(mesh, states, *weights):
+    reps, n, tps = mesh.shape["rep"], mesh.shape["fs"], mesh.shape["tp"]
+    own_width = states.shape[1]
+    channels = own_width * tps
+    planar = (
+        reps == tps == 2
+        and n % tps == 0
+        and n // tps > 2
+        and own_width % (reps * tps * LANES) == 0
+        and channels % (n * LANES) == 0
+        and own_width % (channels // n) == 0
+    )
+    return (plane_body if planar else ring_body)(mesh, states, *weights)
+
+
 def solution(mesh):
     in_specs = (
         P(("rep", "fs"), "tp"),

time: 195 us -> 230 us (1.18)
  Pallas kernels: 191 us -> 227 us
    pallas_call x1, Pallas kernels: 191 us -> 227 us  [plane_body(): pl.pallas_call(functools.partial(plane_kernel, (reps, n, tps, rows, chann...]
where the time goes in v1:
time: 230 us
  Pallas kernels  227 us (99%)
    pallas_call x1, Pallas kernels, plane_body(): pl.pallas_call(functools.partial(plane_kernel, (reps, n, tps, rows, chann...  227 us

profile of v1, /device:TPU:24, one launch (start us, length us, event | category | flops | bytes accessed | tf_op | source)
XLA Modules:
  0.0 229.5 jit_solution(11534758082197990309)
XLA Ops:
  0.0 227.4 %shard_map.100 = bf16[384,1024]{1,0:T(8,128)(2,1)} custom-call(bf16[384,1024]{1,0:T(8,128)(2,1)} %states.1, f32[1,2048]{1,0:T(1,128)} %bitcast.3, bf16[256,1024]{1,0:T(8,128)(2,1)} %w_value.1, bf16[256,1024]{1,0:T(8,128)(2,1)} %w_gate.1, f32[31,2048]{1,0:T(8,128)} %conv_kernel.1, f32[1,2048]{1,0:T(1,128)} %bitcast.4, bf16[256,1024]{1,0:T(8,128)(2,1)} %w_mix.1, ...), custom_call_target="tpu_custom_call" | custom-call | tf_op jit(solution)/shard_map/pallas_call | solution.py:996
  227.4 2.1 copy.12

commit v2 on v1

--- a/solution.py
+++ b/solution.py
@@ -481,10 +481,11 @@
     states, mix_gain, w_value, w_gate, conv_kernel, chan_gain, w_mix, mlp_gain, w_up, w_down,
     out,
     weights, rows_in, rows_mid, normed, padded, filtered, activated, hidden, own_in, own_mid,
-    own_stats, peer_stats, mix_parts, mix_peers, fed_parts, fed_peers,
-    load_sems, y_send, y_recv, near_send, far_send, line_recv, twin_send, twin_recv,
+    own_stats, peer_stats, mix_parts, stage, mix_peers, fed_parts, fed_peers,
+    load_sems, y_send, y_recv, near_send, far_send, line_recv, last_recv,
+    twin_send, twin_recv, last_twin,
     in_send, in_recv, mid_send, mid_recv,
-    stat_send, stat_recv, mix_send, mix_recv, fed_send, fed_recv,
+    stat_send, stat_recv, stage_send, stage_recv, mix_send, mix_recv, fed_send, fed_recv,
 ):
     reps, n, tps, rows, channels, sub, ups = sizes
     ys = tps
@@ -495,7 +496,7 @@
     shard = channels // n
     plane_shard = shard * ys
     tokens = reps * rows
-    pieces = tokens // LENGTH
+    seqs = rows // LENGTH
     chunks = 3 + 2 * ups
     rep, fs, tp = lax.axis_index("rep"), lax.axis_index("fs"), lax.axis_index("tp")
     z, y = fs // ys, lax.rem(fs, ys)
@@ -506,9 +507,20 @@
     blocks, _, block = mix_parts.shape
     per_tp = own_width // block
 
+    third = tuple(range(3, 3 + ups))
+    is_home = tp == y
+    not_home = jnp.logical_not(is_home)
+    fourth = tuple(range(3 + ups, chunks))
+    per_plane = plane_shard // block
     has_next = (z < zs - 1, z > 0)
     next_fs = (fs + ys, fs - ys)
-    is_home = tp == y
+    def scoped(name):
+        def wrap(f):
+            def run(*args):
+                with jax.named_scope("_".join([name, *(str(a) for a in args[:2] if isinstance(a, int))])):
+                    return f(*args)
+            return run
+        return wrap
 
     barrier = pltpu.get_barrier_semaphore()
     for dr in range(reps):
@@ -556,14 +568,14 @@
 
     loads = [
         pltpu.make_async_copy(
-            columns_of(c, own_group), weights.at[c, rows_of(fs), half], load_sems.at[c]
+            columns_of(c, own_group), weights.at[c, rows_of(fs), half], load_sems.at[min(c, 3)]
         )
         for c in range(chunks)
     ]
     home_cols = pl.ds(pl.multiple_of(tp * own_width, own_width), own_width)
-    own_load = pltpu.make_async_copy(states, own_in, load_sems.at[chunks])
+    own_load = pltpu.make_async_copy(states, own_in, load_sems.at[4])
     home_load = pltpu.make_async_copy(
-        states, rows_in.at[rep_rows(rep), home_cols], load_sems.at[chunks + 1]
+        states, rows_in.at[rep_rows(rep), home_cols], load_sems.at[5]
     )
     for c in range(chunks):
         loads[c].start()
@@ -575,108 +587,142 @@
     def across(c):
         return remote(
             columns_of(c, rep * ys + other_y), weights.at[c, rows_of(fs), half],
-            y_send.at[c], y_recv.at[c], fs=other_fs,
+            y_send.at[0], y_recv.at[c], fs=other_fs,
         )
 
     middle = jnp.minimum(z, zs - 1 - z)
 
     def offset_at(i):
-        near = (i + 1) // 2 if i % 2 else -(i // 2)
-        far = jnp.where(2 * z < zs - 1, i - middle, middle - i)
+        low = 2 * z < zs - 1
+        near = -(i + 1) // 2 if i % 2 else i // 2
+        near = jnp.where(low, near, -near)
+        far = jnp.where(low, i - middle, middle - i)
         return jnp.where(i <= 2 * middle, near, far)
 
     offsets = [offset_at(i) for i in range(zs)]
     planes = [z + off for off in offsets]
 
+    def moved(chunk, span, send, recv, **where):
+        at = weights.at[chunk, span, half]
+        return remote(at, at, send, recv, **where)
+
+    def group_of(c):
+        return slice(0, 2) if c < 2 else c if c == 2 else slice(3, 3 + ups)
+
     def twin(c, i):
-        span = rows_of(planes[i], plane_shard)
-        return remote(
-            weights.at[c, span, half], weights.at[c, span, half],
-            twin_send.at[c, i], twin_recv.at[c, i], tp=other_tp,
-        )
-
-    def near(c, way, index):
-        span = rows_of(index)
-        return remote(
-            weights.at[c, span, half], weights.at[c, span, half],
-            near_send.at[c, way], line_recv.at[way, c, 0], fs=next_fs[way],
-        )
-
-    def near_all(c, way):
-        span = rows_of(z, plane_shard)
-        return remote(
-            weights.at[c, span, half], weights.at[c, span, half],
-            near_send.at[c, way], line_recv.at[way, c, 0], fs=next_fs[way],
-        )
-
+        return moved(
+            c, rows_of(planes[i], plane_shard), twin_send.at[c], twin_recv.at[0 if c < 2 else min(c - 1, 2)],
+            tp=other_tp,
+        )
+
+    def twin_last(c, i, b):
+        return moved(
+            c, rows_of(planes[i] * ys + b), twin_send.at[c], last_twin.at[i, b], tp=other_tp
+        )
+
+    def ready(c):
+        group = group_of(c)
+        whole_half = weights.at[group, :, half]
+        remote(
+            whole_half, whole_half, twin_send.at[c], twin_recv.at[0 if c < 2 else min(c - 1, 2)], tp=other_tp
+        ).wait_recv()
+
+    def ready_last(i, b):
+        moved(
+            slice(3 + ups, chunks), rows_of(planes[i] * ys + b), twin_send.at[0],
+            last_twin.at[i, b], tp=other_tp,
+        ).wait_recv()
+
+    def near(c, way, part):
+        recv = last_recv.at[z, part] if c in fourth else line_recv.at[c, z]
+        return moved(c, rows_of(z * ys + part), near_send.at[way], recv, fs=next_fs[way])
+
+    @scoped("begin")
+    def begin(c):
+        if c < 3:
+            loads[c].wait()
+        elif c == 3:
+            at = weights.at[3:, rows_of(fs), half]
+            pltpu.make_async_copy(at, at, load_sems.at[3]).wait()
+        for way in range(2):
+            pl.when(has_next[way])(near(c, way, y).start)
+
+    @scoped("own")
     def own(c):
-        loads[c].wait()
-        for way in range(2):
-            pl.when(has_next[way])(near(c, way, fs).start)
         across(c).wait_recv()
         for way in range(2):
-            pl.when(has_next[way])(near(c, way, other_fs).start)
-        twin(c, 0).start()
-
-    def far(c, i):
-        off, plane = offsets[i], planes[i]
-        upward = off < 0
-        way = jnp.where(upward, 0, 1)
-        step = jnp.abs(off)
-        span = rows_of(plane, plane_shard)
-        arrival = remote(
-            weights.at[c, span, half], weights.at[c, span, half],
-            far_send.at[c, i - 1], line_recv.at[way, c, step - 1], fs=other_fs,
-        )
-        goes = jnp.where(upward, z < zs - 1, z > 0)
-        onward = remote(
-            weights.at[c, span, half], weights.at[c, span, half],
-            far_send.at[c, i - 1], line_recv.at[way, c, jnp.minimum(step, zs - 2)],
-            fs=jnp.where(upward, fs + ys, fs - ys),
-        )
-        return arrival, goes, onward
-
+            pl.when(has_next[way])(near(c, way, other_y).start)
+        if c in fourth:
+            for b in range(ys):
+                twin_last(c, 0, b).start()
+        else:
+            twin(c, 0).start()
+
+    goes = [jnp.where(off < 0, z < zs - 1, z > 0) for off in offsets]
+
+    def onward(chunk, i, span, recv):
+        to = jnp.where(offsets[i] < 0, fs + ys, fs - ys)
+        return moved(chunk, span, far_send.at[i - 1], recv, fs=to)
+
+    @scoped("arrive")
     def arrive(c, i):
-        arrival, goes, onward = far(c, i)
-        arrival.wait_recv()
-        pl.when(goes)(onward.start)
+        copy = onward(c, i, rows_of(planes[i], plane_shard), line_recv.at[c, planes[i]])
+        copy.wait_recv()
+        pl.when(goes[i])(copy.start)
         twin(c, i).start()
 
-    def ready(c, i):
-        twin(c, i).wait_recv()
-
-    def drain(c):
-        across(c).wait_send()
+    @scoped("arrive_last")
+    def arrive_last(i, b):
+        span, recv = rows_of(planes[i] * ys + b), last_recv.at[planes[i], b]
+        copy = onward(slice(3 + ups, chunks), i, span, recv)
+        copy.wait_recv()
+        for c in fourth:
+            pl.when(goes[i])(onward(c, i, span, recv).start)
+        for c in fourth:
+            twin_last(c, i, b).start()
+
+    @scoped("drain")
+    def drain(chunk):
+        moved(chunk, slice(None), twin_send.at[chunk], twin_recv.at[0], tp=other_tp).wait_send()
+
+    @scoped("drain_all")
+    def drain_all():
+        every = slice(None)
+        moved(every, rows_of(fs), y_send.at[0], y_recv.at[0], fs=other_fs).wait_send()
         for way in range(2):
-            pl.when(has_next[way])(near_all(c, way).wait_send)
-        for i in range(zs):
-            twin(c, i).wait_send()
-            if i:
-                _, goes, onward = far(c, i)
-                pl.when(goes)(onward.wait_send)
-
-    def spread(source, target, send, recv):
+            copy = moved(
+                every, rows_of(z, plane_shard), near_send.at[way], y_recv.at[0], fs=next_fs[way]
+            )
+            pl.when(has_next[way])(copy.wait_send)
+        for i in range(1, zs):
+            copy = onward(every, i, rows_of(planes[i], plane_shard), y_recv.at[0])
+            pl.when(goes[i])(copy.wait_send)
+
+    def spread(source, target, send, recv, over_from):
         def at(r, h, j):
             start = pl.multiple_of(h * own_width + j * block, block)
             return target.at[rep_rows(r), pl.ds(start, block)]
 
         def copies(j):
-            src = source.at[:, j * block : (j + 1) * block]
-            dst = at(rep, tp, j)
-            along = remote(src, dst, send.at[0, j], recv.at[1, tp, j], rep=other_rep, tp=y)
-            over = remote(src, dst, send.at[1, j], recv.at[0, tp, j], fs=other_fs, tp=y)
-            inside = remote(src, dst, send.at[2, j], recv.at[0, tp, j], tp=y)
+            if isinstance(j, slice):
+                src, dst, j = source, target.at[rep_rows(rep), home_cols], 0
+            else:
+                src, dst = source.at[:, j * block : (j + 1) * block], at(rep, tp, j)
+            along = remote(src, dst, send.at[0], recv.at[1, tp, j], rep=other_rep, tp=y)
+            over = remote(src, dst, send.at[1], recv.at[0, tp, j], fs=other_fs, tp=y)
+            inside = remote(src, dst, send.at[2], recv.at[0, tp, j], tp=y)
             return along, over, inside
 
-        def passing(j):
-            one, two = at(other_rep, 0, j), at(rep, 1, j)
-            over = remote(one, one, send.at[3, j], recv.at[1, 0, j], fs=other_fs)
-            along = remote(two, two, send.at[3, j], recv.at[1, 1, j], rep=other_rep)
-            return over, along
+        def passing(h, j):
+            if h == 0 and j >= over_from:
+                one = at(other_rep, 0, j)
+                return remote(one, one, send.at[3], recv.at[1, 0, j], fs=other_fs)
+            two = at(rep, h, j)
+            return remote(two, two, send.at[3 + h], recv.at[1, h, j], rep=other_rep)
 
         def arrival(dr, h, j):
             dst = at(rep if dr == 0 else other_rep, h, j)
-            return remote(dst, dst, send.at[0, j], recv.at[dr, h, j], rep=other_rep)
+            return remote(dst, dst, send.at[0], recv.at[dr, h, j], rep=other_rep)
 
         def start(j):
             along, over, inside = copies(j)
@@ -684,40 +730,58 @@
             over.start()
             pl.when(jnp.logical_not(is_home))(inside.start)
 
+        @scoped("forward")
         def forward(j):
-            over, along = passing(j)
-
-            @pl.when(is_home)
-            def _():
-                arrival(1, 0, j).wait_recv()
-                over.start()
+            if j >= over_from:
+                @pl.when(is_home)
+                def _():
+                    arrival(1, 0, j).wait_recv()
+                    passing(0, j).start()
 
             @pl.when(jnp.logical_not(is_home))
             def _():
-                arrival(0, 1, j).wait_recv()
-                along.start()
-
+                for h in range(tps):
+                    if h or j < over_from:
+                        arrival(0, h, j).wait_recv()
+                        passing(h, j).start()
+
+        @scoped("finish")
         def finish(j):
             arrival(1, 1, j).wait_recv()
 
             @pl.when(is_home)
             def _():
                 arrival(0, other_tp, j).wait_recv()
+                if j < over_from:
+                    arrival(1, 0, j).wait_recv()
 
             @pl.when(jnp.logical_not(is_home))
             def _():
-                arrival(0, 0, j).wait_recv()
                 arrival(1, 0, j).wait_recv()
-
-        def settle(j):
-            along, over, inside = copies(j)
+                if j >= over_from:
+                    arrival(0, 0, j).wait_recv()
+
+        def settle():
+            along, over, inside = copies(slice(None))
             along.wait_send()
             over.wait_send()
-            pl.when(jnp.logical_not(is_home))(inside.wait_send)
-            passing(j)[0].wait_send()
+            pl.when(not_home)(inside.wait_send)
+
+            def part(k, blocks_sent):
+                if blocks_sent:
+                    sent = target.at[rep_rows(rep), : blocks_sent * block]
+                    remote(sent, sent, send.at[k], recv.at[0, 0, 0], fs=other_fs).wait_send()
+
+            pl.when(is_home)(functools.partial(part, 3, per_tp - over_from))
+
+            @pl.when(not_home)
+            def _():
+                part(3, over_from)
+                part(4, per_tp)
 
         return start, forward, finish, settle
 
+    @scoped("norm")
     def norm_all(source, gain):
         def one(i, carry):
             span = pl.ds(pl.multiple_of(i * 64, 64), 64)
@@ -759,22 +823,27 @@
             jnp.sum(one, axis=-1, keepdims=True),
             jnp.where(lane == 1, jnp.sum(two, axis=-1, keepdims=True), 0.0),
         )
-        own_stats[:, seq_rows(i)] = both.T[0:8, :]
-
-    def stat_copies():
+        own_stats[i // seqs, :, seq_rows(lax.rem(i, seqs))] = both.T[0:8, :]
+
+    def stat_copies(r):
         return [
             remote(
-                own_stats, peer_stats.at[dr * ys + dy], stat_send.at[dr, dy],
-                stat_recv.at[dr, dy],
+                own_stats.at[r], peer_stats.at[dr * ys + dy, r], stat_send.at[r],
+                stat_recv.at[r],
                 rep=lax.rem(rep + dr, reps), fs=z * ys + lax.rem(y + dy, ys),
             )
             for dr in range(reps) for dy in range(ys) if dr or dy
         ]
 
+    def stat_waits(r):
+        at = peer_stats.at[1:, r]
+        return remote(at, at, stat_send.at[r], stat_recv.at[r], rep=other_rep)
+
     def activate_rows(i, carry):
-        total = own_stats[:, seq_rows(i)]
+        within = seq_rows(lax.rem(i, seqs))
+        total = own_stats[i // seqs, :, within]
         for k in range(1, members):
-            total = total + peer_stats[k, :, seq_rows(i)]
+            total = total + peer_stats[k, i // seqs, :, within]
         turned = jnp.concatenate([total] * (LANES // 8), axis=0).T
         mean = turned[:, 0:1] / channels
         variance = turned[:, 1:2] / channels - mean * mean
@@ -789,49 +858,137 @@
         activated[seq_rows(i), :] = (x / (1.0 + jnp.exp(-x))).astype(jnp.bfloat16)
         return carry
 
-    def share(order, o, left, pieces_of, parts, peers, send, recv):
+    @scoped("share")
+    def share(o, dr, left, pieces_of, parts, peers, send, recv):
+        to = lax.rem(rep + dr, reps)
         span = rows_of(o, block)
         keeper, kept = o // per_tp, lax.rem(o, per_tp)
-        waits = []
-        for dr in [*range(1, reps), 0]:
-            to = lax.rem(rep + dr, reps)
-            at = rep_rows(to)
-            total = None
-            for k, c in enumerate(pieces_of):
-                term = times_transposed(
-                    left[at, k * width : (k + 1) * width], weights[c, span, :]
-                )
-                total = term if total is None else total + term
-            parts[o, at, :] = total.astype(jnp.bfloat16)
-            slot = (reps - dr) % reps * ys + lax.rem(y + ys - tp, ys)
-            copy = remote(
-                parts.at[o, at, :], peers.at[slot, kept], send.at[order, dr],
-                recv.at[slot, kept], rep=to, fs=z * ys + tp, tp=keeper,
+        at = rep_rows(to)
+        total = None
+        for k, c in enumerate(pieces_of):
+            term = times_transposed(left[at, k * width : (k + 1) * width], weights[c, span, :])
+            total = term if total is None else total + term
+        parts[o, at, :] = total.astype(jnp.bfloat16)
+        slot = lax.rem(rep + reps - to, reps) * ys + lax.rem(y + ys - tp, ys)
+        copy = remote(
+            parts.at[o, at, :], peers.at[slot, kept], send.at[dr], recv.at[kept],
+            rep=to, fs=z * ys + tp, tp=keeper,
+        )
+        here = jnp.logical_and(is_home, jnp.logical_and(keeper == tp, to == rep))
+        pl.when(jnp.logical_not(here))(copy.start)
+
+    def along_first(o):
+        return o % 2 == 0
+
+    def stage_copy(o, r):
+        if along_first(o):
+            return remote(
+                mix_parts.at[o, rep_rows(other_rep), :], stage.at[o, 0], stage_send.at[0],
+                stage_recv.at[o], rep=other_rep,
             )
-            if dr:
-                copy.start()
-                waits.append(copy.wait_send)
-            else:
-                away = jnp.logical_not(jnp.logical_and(is_home, keeper == tp))
-                pl.when(away)(copy.start)
-                waits.append(lambda w=away, c=copy: pl.when(w)(c.wait_send))
-        return waits
-
+        return remote(
+            mix_parts.at[o, rep_rows(r), :], stage.at[o, r], stage_send.at[1],
+            stage_recv.at[o], fs=z * ys + tp,
+        )
+
+    def last_copies(o):
+        keeper, kept = o // per_tp, o % per_tp
+        own_part = mix_parts.at[o, rep_rows(rep), :]
+        inside = remote(
+            own_part, mix_peers.at[0, kept], mix_send.at[0], mix_recv.at[kept], tp=keeper
+        )
+        if along_first(o):
+            outside = remote(
+                own_part, mix_peers.at[1, kept], mix_send.at[1], mix_recv.at[kept],
+                fs=z * ys + tp, tp=keeper,
+            )
+        else:
+            outside = remote(
+                mix_parts.at[o, rep_rows(other_rep), :], mix_peers.at[1, kept],
+                mix_send.at[1], mix_recv.at[kept], rep=other_rep, tp=keeper,
+            )
+        inner_one = jnp.logical_and(is_home, tp != keeper)
+        return inside, inner_one, outside, not_home if along_first(o) else is_home
+
+    @scoped("mix_share")
+    def mix_share(o, r):
+        at = rep_rows(r)
+        mix_parts[o, at, :] = times_transposed(
+            activated[at, :], weights[2, o * block : (o + 1) * block, :]
+        ).astype(jnp.bfloat16)
+        pl.when(rep != r if along_first(o) else not_home)(stage_copy(o, r).start)
+
+    def mix_add(o, at, k):
+        total = mix_parts[o, at, :].astype(jnp.float32) + stage[o, k].astype(jnp.float32)
+        mix_parts[o, at, :] = total.astype(jnp.bfloat16)
+
+    @scoped("combine")
+    def combine(o):
+        keeper, kept = o // per_tp, o % per_tp
+        inside, inner_one, outside, outer_one = last_copies(o)
+
+        def pass_on():
+            pl.when(outer_one)(outside.start)
+            pl.when(inner_one)(inside.start)
+
+            @pl.when(jnp.logical_and(is_home, tp == keeper))
+            def _():
+                mix_peers[0, kept] = mix_parts[o, rep_rows(rep), :]
+
+        if along_first(o):
+            stage_copy(o, 0).wait_recv()
+            mix_add(o, rep_rows(rep), 0)
+            pass_on()
+        else:
+            @pl.when(is_home)
+            def _():
+                both = stage.at[o]
+                remote(both, both, stage_send.at[1], stage_recv.at[o], fs=other_fs).wait_recv()
+                for r in range(reps):
+                    mix_add(o, rep_rows(r), r)
+                pass_on()
+
+    @scoped("mix_final")
+    def mix_final(j):
+        def some(start):
+            at = mix_peers.at[start:, j]
+            return remote(at, at, mix_send.at[0], mix_recv.at[j], rep=other_rep)
+
+        pl.when(is_home)(some(1).wait_recv)
+        pl.when(not_home)(some(0).wait_recv)
+        return mix_peers[0, j].astype(jnp.float32) + mix_peers[1, j].astype(jnp.float32)
+
+    def mix_settle():
+        def sent(count, send):
+            at = mix_parts.at[:count, rep_rows(rep), :]
+            return remote(at, at, send, mix_recv.at[0], rep=other_rep)
+
+        even = sum(1 for o in range(blocks) if along_first(o))
+        sent(even, stage_send.at[0]).wait_send()
+        pl.when(not_home)(sent((blocks - even) * reps, stage_send.at[1]).wait_send)
+        pl.when(is_home)(sent(per_tp, mix_send.at[0]).wait_send)
+        pl.when(not_home)(sent(even, mix_send.at[1]).wait_send)
+        pl.when(is_home)(sent(blocks - even, mix_send.at[1]).wait_send)
+
+    @scoped("peers")
     def wait_peers(j, parts, peers, send, recv):
-        def one(k):
-            return remote(
-                parts.at[0, rep_rows(rep), :], peers.at[k, j], send.at[0, 0], recv.at[k, j],
-                rep=other_rep,
-            )
-
-        for k in range(1, members):
-            one(k).wait_recv()
+        def some(start):
+            at = peers.at[start:, j]
+            return remote(at, at, send.at[0], recv.at[j], rep=other_rep)
 
         @pl.when(is_home)
         def _():
             peers[0, j] = parts[tp * per_tp + j, rep_rows(rep), :]
-
-        pl.when(jnp.logical_not(is_home))(one(0).wait_recv)
+            some(1).wait_recv()
+
+        pl.when(not_home)(some(0).wait_recv)
+
+    def settle_share(parts, send, recv):
+        for dr in range(reps):
+            for count, who in ((per_tp, is_home), (blocks, not_home)):
+                sent = parts.at[: count if dr == 0 else blocks, rep_rows(rep), :]
+                copy = remote(sent, sent, send.at[dr], recv.at[0], rep=other_rep)
+                pl.when(who)(copy.wait_send)
 
     def total_of(j, peers):
         total = peers[0, j].astype(jnp.float32)
@@ -839,85 +996,115 @@
             total = total + peers[k, j].astype(jnp.float32)
         return total
 
-    third = tuple(range(3, 3 + ups))
-    fourth = tuple(range(3 + ups, chunks))
-    per_plane = plane_shard // block
-
-    start_in, forward_in, finish_in, settle_in = spread(states, rows_in, in_send, in_recv)
-    start_mid, forward_mid, finish_mid, settle_mid = spread(own_mid, rows_mid, mid_send, mid_recv)
+    start_in, forward_in, finish_in, settle_in = spread(
+        states, rows_in, in_send, in_recv, per_tp // 2
+    )
+    start_mid, forward_mid, finish_mid, settle_mid = spread(
+        own_mid, rows_mid, mid_send, mid_recv, 0
+    )
+
+    def inner(*todo):
+        @pl.when(middle > 0)
+        def _():
+            for one in todo:
+                one()
+
+    def outer(*todo):
+        @pl.when(middle == 0)
+        def _():
+            for one in todo:
+                one()
+
+    def pump(c, i):
+        return functools.partial(arrive, c, i)
+
+    def all_of(c):
+        return [pump(c, i) for i in range(1, zs)]
+
+    def whole(c):
+        return [functools.partial(begin, c), functools.partial(own, c)]
 
     across(0).start()
     across(1).start()
-    own(0)
+    begin(0)
+    begin(1)
     for j in range(per_tp):
         start_in(j)
+    own(0)
     own(1)
-    for c in range(2, chunks):
-        across(c).start()
+    across(2).start()
+    across(3).start()
     padded[0:LEAD, :] = jnp.zeros((LEAD, width), jnp.float32)
     arrive(0, 1)
-    for j in range(per_tp // 2):
+    arrive(1, 1)
+    forward_in(0)
+    inner(pump(0, 2), pump(1, 2))
+    for j in range(1, per_tp // 2):
         forward_in(j)
-    arrive(0, 2)
+    inner(*[pump(c, i) for i in range(3, zs) for c in (0, 1)])
     for j in range(per_tp // 2, per_tp):
         forward_in(j)
-    arrive(0, 3)
+    begin(2)
     own(2)
-    pl.when(is_home)(home_load.wait)
-    arrive(1, 1)
+    outer(*[pump(c, 2) for c in (0, 1)])
     for j in range(per_tp):
         finish_in(j)
+    for c in range(4, chunks):
+        across(c).start()
+    pl.when(is_home)(home_load.wait)
     norm_all(rows_in, mix_gain)
-    arrive(1, 2)
-    own(3)
-    arrive(1, 3)
-    for c in (0, 1):
-        for i in range(zs):
-            ready(c, i)
-
-    todo = [functools.partial(arrive, 2, i) for i in range(1, zs)]
-    todo.append(functools.partial(own, 4))
-    for i in range(0, pieces, 2):
-        lax.fori_loop(
-            i, min(i + 2, pieces), lambda k, carry: (mixer_rows(k), carry)[1], 0
-        )
-        if todo:
-            todo.pop(0)()
-    stats = stat_copies()
-    for one in stats:
-        one.start()
-    while todo:
-        todo.pop(0)()
-    for one in stats:
-        one.wait_recv()
-    lax.fori_loop(0, pieces, activate_rows, 0)
-    waits = []
-    mix = (activated, (2,), mix_parts, mix_peers, mix_send, mix_recv)
-    for i in range(zs):
-        ready(2, i)
-        for b in range(per_plane):
-            waits += share(len(waits) // reps, planes[i] * per_plane + b, *mix)
-
-    todo = [functools.partial(arrive, 3, i) for i in range(1, zs)]
-    for c in range(4, 3 + ups):
-        todo.append(functools.partial(own, c + 1))
-        todo += [functools.partial(arrive, c, i) for i in range(1, zs)]
-    todo += [functools.partial(own, c) for c in range(4 + ups, chunks)]
-    steps = 2 * per_tp + 1
-    cuts = [len(todo) * k // steps for k in range(steps + 1)]
-
-    def do_some(k):
-        for one in todo[cuts[k] : cuts[k + 1]]:
-            one()
+    outer(*[pump(c, i) for i in range(3, zs) for c in (0, 1)])
+    ready(0)
+
+    inner(*all_of(2)[:1])
+    outer(*whole(3))
+    inside = [
+        all_of(2)[1:2], whole(3), all_of(2)[2:], whole(4),
+    ]
+    outside = [whole(4), whole(5), whole(fourth[0]), sum([whole(c) for c in fourth[1:]], [])]
+    for r in range(reps):
+        for cut in ((0, (seqs + 1) // 2), ((seqs + 1) // 2, seqs)):
+            with jax.named_scope("mixer"):
+                lax.fori_loop(
+                    r * seqs + cut[0], r * seqs + cut[1],
+                    lambda k, carry: (mixer_rows(k), carry)[1], 0,
+                )
+            if inside:
+                inner(*inside.pop(0))
+                outer(*outside.pop(0))
+        for one in stat_copies(r):
+            one.start()
+    outer(*all_of(2))
+    ready(2)
+    for r in range(reps):
+        with jax.named_scope("stats"):
+            stat_waits(r).wait_recv()
+        with jax.named_scope("activate"):
+            lax.fori_loop(r * seqs, (r + 1) * seqs, activate_rows, 0)
+        for j in range(per_tp):
+            for t in range(tps):
+                mix_share(t * per_tp + j, r)
 
     own_load.wait()
-    do_some(0)
+    inner(*whole(5), *all_of(3)[:2])
+    def last(i, b):
+        return [functools.partial(arrive_last, i, b)]
+
+    early = [
+        all_of(3)[2:] + all_of(4)[:2],
+        all_of(4)[2:] + all_of(5)[:2] + whole(fourth[0]),
+        all_of(5)[2:] + sum([whole(c) for c in fourth[1:]], []),
+    ]
+    late = [[], all_of(3), all_of(4)[:1], all_of(4)[1:]]
+    for t in range(tps):
+        combine(t * per_tp)
     for j in range(per_tp):
-        wait_peers(j, mix_parts, mix_peers, mix_send, mix_recv)
+        if j + 1 < per_tp:
+            for t in range(tps):
+                combine(t * per_tp + j + 1)
+        mixed = mix_final(j)
         cols = slice(j * block, (j + 1) * block)
-        own_mid[:, cols] = (
-            own_in[:, cols].astype(jnp.float32) + total_of(j, mix_peers)
-        ).astype(jnp.bfloat16)
+        own_mid[:, cols] = (own_in[:, cols].astype(jnp.float32) + mixed).astype(jnp.bfloat16)
         start_mid(j)
 
         @pl.when(is_home)
@@ -925,18 +1112,26 @@
             start = pl.multiple_of(tp * own_width + j * block, block)
             rows_mid[rep_rows(rep), pl.ds(start, block)] = own_mid[:, cols]
 
-        do_some(1 + j)
         if j:
             forward_mid(j - 1)
-    forward_mid(per_tp - 1)
+        if j < len(early):
+            inner(*early[j])
+        if j == per_tp - 1:
+            forward_mid(j)
+            inner(*[one for b in range(ys) for one in last(1, b)])
+        if j < len(late):
+            outer(*late[j])
+    for rest in early[per_tp:]:
+        inner(*rest)
+    for rest in late[per_tp:]:
+        outer(*rest)
     for j in range(per_tp):
-        do_some(1 + per_tp + j)
         finish_mid(j)
+    outer(*all_of(5))
     norm_all(rows_mid, mlp_gain)
-    for c in third:
-        for i in range(zs):
-            ready(c, i)
-
+    ready(3)
+
+    @scoped("up")
     def up_some(k):
         def up_rows(i, carry):
             at = rep_rows(i)
@@ -949,32 +1144,37 @@
 
     for k in range(ups):
         up_some(k)
-        arrive(fourth[k], 1)
-    done = []
     fed = (hidden, fourth, fed_parts, fed_peers, fed_send, fed_recv)
+    settle_in()
+    settle_mid()
+    mix_settle()
+    for r in range(reps):
+        stat_waits(r).wait_send()
     for i in range(zs):
-        if i > 1:
+        for b in range(ys):
+            if i:
+                outer(*last(i, b))
+            if 1 < i + 1 < zs:
+                inner(*last(i + 1, b))
+            ready_last(i, b)
+            for dr in (*range(1, reps), 0):
+                share(planes[i] * ys + b, dr, *fed)
+            if i == 1 and b == 0:
+                for c in range(3 + ups):
+                    drain(c)
+    for j in range(per_tp):
+        if j == per_tp - 1:
             for c in fourth:
-                arrive(c, i)
-        for c in fourth:
-            ready(c, i)
-        for b in range(per_plane):
-            done += share(len(done) // reps, planes[i] * per_plane + b, *fed)
-    for j in range(per_tp):
+                drain(c)
+            drain_all()
         wait_peers(j, fed_parts, fed_peers, fed_send, fed_recv)
         cols = slice(j * block, (j + 1) * block)
-        out[:, cols] = (
-            own_mid[:, cols].astype(jnp.float32) + total_of(j, fed_peers)
-        ).astype(jnp.bfloat16)
-    for one in stats:
-        one.wait_send()
-    for j in range(per_tp):
-        settle_in(j)
-        settle_mid(j)
-    for c in range(chunks):
-        drain(c)
-    for wait in waits + done:
-        wait()
+        with jax.named_scope("out"):
+            out[:, cols] = (
+                own_mid[:, cols].astype(jnp.float32) + total_of(j, fed_peers)
+            ).astype(jnp.bfloat16)
+    with jax.named_scope("done"):
+        settle_share(fed_parts, fed_send, fed_recv)
 
 
 def plane_body(mesh, states, mix_gain, w_value, w_gate, conv_kernel, chan_gain, w_mix, mlp_gain, w_up, w_down):
@@ -1009,30 +1209,35 @@
             pltpu.VMEM((tokens, ups * width), bf16),
             pltpu.VMEM((rows, own_width), bf16),
             pltpu.VMEM((rows, own_width), bf16),
-            pltpu.VMEM((8, tokens), f32),
-            pltpu.VMEM((members, 8, tokens), f32),
+            pltpu.VMEM((reps, 8, rows), f32),
+            pltpu.VMEM((members, reps, 8, rows), f32),
+            pltpu.VMEM((blocks, tokens, block), bf16),
+            pltpu.VMEM((blocks, reps, rows, block), bf16),
+            pltpu.VMEM((2, per_tp, rows, block), bf16),
             pltpu.VMEM((blocks, tokens, block), bf16),
             pltpu.VMEM((members, per_tp, rows, block), bf16),
-            pltpu.VMEM((blocks, tokens, block), bf16),
-            pltpu.VMEM((members, per_tp, rows, block), bf16),
-            dma((chunks + 2,)),
+            dma((6,)),
+            dma((1,)),
             dma((chunks,)),
+            dma((2,)),
+            dma((zs - 1,)),
+            dma((3 + ups, zs)),
+            dma((zs, ys)),
             dma((chunks,)),
-            dma((chunks, 2)),
-            dma((chunks, zs - 1)),
-            dma((2, chunks, zs - 1)),
-            dma((chunks, zs)),
-            dma((chunks, zs)),
-            dma((4, per_tp)),
+            dma((3,)),
+            dma((zs, ys)),
+            dma((5,)),
             dma((reps, tps, per_tp)),
-            dma((4, per_tp)),
+            dma((5,)),
             dma((reps, tps, per_tp)),
-            dma((reps, ys)),
-            dma((reps, ys)),
-            dma((blocks, reps)),
-            dma((members, per_tp)),
-            dma((blocks, reps)),
-            dma((members, per_tp)),
+            dma((reps,)),
+            dma((reps,)),
+            dma((2,)),
+            dma((blocks,)),
+            dma((2,)),
+            dma((per_tp,)),
+            dma((reps,)),
+            dma((per_tp,)),
         ],
         compiler_params=pltpu.CompilerParams(
             collective_id=0, has_side_effects=True, vmem_limit_bytes=62 * 1024 * 1024

time: 230 us -> 174 us (0.76)
  Pallas kernels: 227 us -> 171 us
    pallas_call x1, Pallas kernels: 227 us -> 171 us  [plane_body(): pl.pallas_call(functools.partial(plane_kernel, (reps, n, tps, rows, chann...]
where the time goes in v2:
time: 174 us; the launch traced here: 173 us
  Pallas kernels  171 us (98%)
  local copies, waits for them, and re-layouts  2.06 us (1%)
    pallas_call x1, Pallas kernels, plane_body(): pl.pallas_call(functools.partial(plane_kernel, (reps, n, tps, rows, chann...  171 us

profile of v2, /device:TPU:24, one launch (start us, length us, event | category | flops | bytes accessed | tf_op | source)
XLA Modules:
  0.0 173.3 jit_solution(5110709496259124893)
XLA Ops:
  0.0 171.2 %shard_map.100 = bf16[384,1024]{1,0:T(8,128)(2,1)} custom-call(bf16[384,1024]{1,0:T(8,128)(2,1)} %states.1, f32[1,2048]{1,0:T(1,128)} %bitcast.3, bf16[256,1024]{1,0:T(8,128)(2,1)} %w_value.1, bf16[256,1024]{1,0:T(8,128)(2,1)} %w_gate.1, f32[31,2048]{1,0:T(8,128)} %conv_kernel.1, f32[1,2048]{1,0:T(1,128)} %bitcast.4, bf16[256,1024]{1,0:T(8,128)(2,1)} %w_mix.1, ...), custom_call_target="tpu_custom_call" | custom-call | tf_op jit(solution)/shard_map/pallas_call | solution.py:1196
  171.2 2.1 %copy.12 = bf16[384,1024]{1,0:T(8,128)(2,1)} copy(bf16[384,1024]{1,0:T(8,128)(2,1)} %shard_map.100) | data formatting | bytes 1572864

commit v3 on v2

--- a/solution.py
+++ b/solution.py
@@ -478,8 +478,9 @@
 
 def plane_kernel(
     sizes,
-    states, mix_gain, w_value, w_gate, conv_kernel, chan_gain, w_mix, mlp_gain, w_up, w_down,
+    states, mix_gain_in, w_value, w_gate, taps_in, chan_gain_in, w_mix, mlp_gain_in, w_up, w_down,
     out,
+    mix_gain, conv_kernel, chan_gain, mlp_gain,
     weights, rows_in, rows_mid, normed, padded, filtered, activated, hidden, own_in, own_mid,
     own_stats, peer_stats, mix_parts, stage, mix_peers, fed_parts, fed_peers,
     load_sems, y_send, y_recv, near_send, far_send, line_recv, last_recv,
@@ -577,10 +578,21 @@
     home_load = pltpu.make_async_copy(
         states, rows_in.at[rep_rows(rep), home_cols], load_sems.at[5]
     )
+    small_loads = [
+        pltpu.make_async_copy(source, target, load_sems.at[6 + k])
+        for k, (source, target) in enumerate(
+            (
+                (mix_gain_in, mix_gain), (taps_in, conv_kernel), (chan_gain_in, chan_gain),
+                (mlp_gain_in, mlp_gain),
+            )
+        )
+    ]
     for c in range(chunks):
         loads[c].start()
     pl.when(is_home)(home_load.start)
     own_load.start()
+    for one in small_loads:
+        one.start()
     along_line = sum(jnp.where(has, 1, 0) for has in has_next)
     pl.semaphore_wait(barrier, reps * ys * tps - 1 + along_line)
 
@@ -615,9 +627,15 @@
             tp=other_tp,
         )
 
-    def twin_last(c, i, b):
+    halves = shard // LANES
+
+    def half_rows(index, h):
+        return rows_of(index * halves + h, LANES)
+
+    def twin_last(c, i, b, h):
         return moved(
-            c, rows_of(planes[i] * ys + b), twin_send.at[c], last_twin.at[i, b], tp=other_tp
+            c, half_rows(planes[i] * ys + b, h), twin_send.at[c], last_twin.at[i, b, h],
+            tp=other_tp,
         )
 
     def ready(c):
@@ -627,15 +645,32 @@
             whole_half, whole_half, twin_send.at[c], twin_recv.at[0 if c < 2 else min(c - 1, 2)], tp=other_tp
         ).wait_recv()
 
-    def ready_last(i, b):
+    def ready_last(i, b, h):
         moved(
-            slice(3 + ups, chunks), rows_of(planes[i] * ys + b), twin_send.at[0],
-            last_twin.at[i, b], tp=other_tp,
+            slice(3 + ups, chunks), half_rows(planes[i] * ys + b, h), twin_send.at[0],
+            last_twin.at[i, b, h], tp=other_tp,
         ).wait_recv()
 
     def near(c, way, part):
-        recv = last_recv.at[z, part] if c in fourth else line_recv.at[c, z]
-        return moved(c, rows_of(z * ys + part), near_send.at[way], recv, fs=next_fs[way])
+        if c not in fourth:
+            return [
+                moved(
+                    c, rows_of(z * ys + part), near_send.at[way], line_recv.at[c, z],
+                    fs=next_fs[way],
+                )
+            ]
+        return [
+            moved(
+                c, half_rows(z * ys + part, h), near_send.at[way], last_recv.at[z, part, h],
+                fs=next_fs[way],
+            )
+            for h in range(halves)
+        ]
+
+    def send_near(c, part):
+        for way in range(2):
+            for one in near(c, way, part):
+                pl.when(has_next[way])(one.start)
 
     @scoped("begin")
     def begin(c):
@@ -644,17 +679,16 @@
         elif c == 3:
             at = weights.at[3:, rows_of(fs), half]
             pltpu.make_async_copy(at, at, load_sems.at[3]).wait()
-        for way in range(2):
-            pl.when(has_next[way])(near(c, way, y).start)
+        send_near(c, y)
 
     @scoped("own")
     def own(c):
         across(c).wait_recv()
-        for way in range(2):
-            pl.when(has_next[way])(near(c, way, other_y).start)
+        send_near(c, other_y)
         if c in fourth:
             for b in range(ys):
-                twin_last(c, 0, b).start()
+                for h in range(halves):
+                    twin_last(c, 0, b, h).start()
         else:
             twin(c, 0).start()
 
@@ -672,14 +706,14 @@
         twin(c, i).start()
 
     @scoped("arrive_last")
-    def arrive_last(i, b):
-        span, recv = rows_of(planes[i] * ys + b), last_recv.at[planes[i], b]
+    def arrive_last(i, b, h):
+        span, recv = half_rows(planes[i] * ys + b, h), last_recv.at[planes[i], b, h]
         copy = onward(slice(3 + ups, chunks), i, span, recv)
         copy.wait_recv()
         for c in fourth:
             pl.when(goes[i])(onward(c, i, span, recv).start)
         for c in fourth:
-            twin_last(c, i, b).start()
+            twin_last(c, i, b, h).start()
 
     @scoped("drain")
     def drain(chunk):
@@ -859,19 +893,21 @@
         return carry
 
     @scoped("share")
-    def share(o, dr, left, pieces_of, parts, peers, send, recv):
+    def share(o, dr, part, left, pieces_of, parts, peers, send, recv):
         to = lax.rem(rep + dr, reps)
-        span = rows_of(o, block)
+        first, size = part
+        span = pl.ds(pl.multiple_of(o * block + first, size), size)
+        cols = pl.ds(first, size)
         keeper, kept = o // per_tp, lax.rem(o, per_tp)
         at = rep_rows(to)
         total = None
         for k, c in enumerate(pieces_of):
             term = times_transposed(left[at, k * width : (k + 1) * width], weights[c, span, :])
             total = term if total is None else total + term
-        parts[o, at, :] = total.astype(jnp.bfloat16)
+        parts[o, at, cols] = total.astype(jnp.bfloat16)
         slot = lax.rem(rep + reps - to, reps) * ys + lax.rem(y + ys - tp, ys)
         copy = remote(
-            parts.at[o, at, :], peers.at[slot, kept], send.at[dr], recv.at[kept],
+            parts.at[o, at, cols], peers.at[slot, kept, :, cols], send.at[dr], recv.at[kept],
             rep=to, fs=z * ys + tp, tp=keeper,
         )
         here = jnp.logical_and(is_home, jnp.logical_and(keeper == tp, to == rep))
@@ -1052,6 +1088,8 @@
     for c in range(4, chunks):
         across(c).start()
     pl.when(is_home)(home_load.wait)
+    for one in small_loads:
+        one.wait()
     norm_all(rows_in, mix_gain)
     outer(*[pump(c, i) for i in range(3, zs) for c in (0, 1)])
     ready(0)
@@ -1059,7 +1097,7 @@
     inner(*all_of(2)[:1])
     outer(*whole(3))
     inside = [
-        all_of(2)[1:2], whole(3), all_of(2)[2:], whole(4),
+        all_of(2)[1:2], all_of(2)[2:] + whole(3), whole(4), [],
     ]
     outside = [whole(4), whole(5), whole(fourth[0]), sum([whole(c) for c in fourth[1:]], [])]
     for r in range(reps):
@@ -1088,7 +1126,7 @@
     own_load.wait()
     inner(*whole(5), *all_of(3)[:2])
     def last(i, b):
-        return [functools.partial(arrive_last, i, b)]
+        return [functools.partial(arrive_last, i, b, h) for h in range(halves)]
 
     early = [
         all_of(3)[2:] + all_of(4)[:2],
@@ -1152,13 +1190,21 @@
         stat_waits(r).wait_send()
     for i in range(zs):
         for b in range(ys):
-            if i:
-                outer(*last(i, b))
             if 1 < i + 1 < zs:
                 inner(*last(i + 1, b))
-            ready_last(i, b)
-            for dr in (*range(1, reps), 0):
-                share(planes[i] * ys + b, dr, *fed)
+            if i < zs - 1:
+                if i:
+                    outer(*last(i, b))
+                for h in range(halves):
+                    ready_last(i, b, h)
+                for dr in (*range(1, reps), 0):
+                    share(planes[i] * ys + b, dr, (0, block), *fed)
+            else:
+                for h in range(halves):
+                    outer(last(i, b)[h])
+                    ready_last(i, b, h)
+                    for dr in (*range(1, reps), 0):
+                        share(planes[i] * ys + b, dr, (h * LANES, LANES), *fed)
             if i == 1 and b == 0:
                 for c in range(3 + ups):
                     drain(c)
@@ -1188,6 +1234,7 @@
     ups = w_up.shape[1] // own_width
     tokens = rows * reps
     block = channels // n
+    halves = block // LANES
     blocks, per_tp = channels // block, own_width // block
     chunks = 3 + 2 * ups
     bf16, f32 = jnp.bfloat16, jnp.float32
@@ -1195,10 +1242,14 @@
     dma = pltpu.SemaphoreType.DMA
     return pl.pallas_call(
         functools.partial(plane_kernel, (reps, n, tps, rows, channels, sub, ups)),
-        out_shape=jax.ShapeDtypeStruct((rows, own_width), bf16),
-        in_specs=[hbm, vmem, hbm, hbm, vmem, vmem, hbm, vmem, hbm, hbm],
+        out_shape=pltpu.VMEM((rows, own_width), bf16),
+        in_specs=[hbm] * 10,
         out_specs=vmem,
         scratch_shapes=[
+            pltpu.VMEM((1, channels), f32),
+            pltpu.VMEM(conv_kernel.shape, f32),
+            pltpu.VMEM((1, channels), f32),
+            pltpu.VMEM((1, channels), f32),
             pltpu.VMEM((chunks, channels, width), bf16),
             pltpu.VMEM((tokens, channels), bf16),
             pltpu.VMEM((tokens, channels), bf16),
@@ -1216,16 +1267,16 @@
             pltpu.VMEM((2, per_tp, rows, block), bf16),
             pltpu.VMEM((blocks, tokens, block), bf16),
             pltpu.VMEM((members, per_tp, rows, block), bf16),
-            dma((6,)),
+            dma((10,)),
             dma((1,)),
             dma((chunks,)),
             dma((2,)),
             dma((zs - 1,)),
             dma((3 + ups, zs)),
-            dma((zs, ys)),
+            dma((zs, ys, halves)),
             dma((chunks,)),
             dma((3,)),
-            dma((zs, ys)),
+            dma((zs, ys, halves)),
             dma((5,)),
             dma((reps, tps, per_tp)),
             dma((5,)),
@@ -1240,7 +1291,7 @@
             dma((per_tp,)),
         ],
         compiler_params=pltpu.CompilerParams(
-            collective_id=0, has_side_effects=True, vmem_limit_bytes=62 * 1024 * 1024
+            collective_id=0, has_side_effects=True, vmem_limit_bytes=56 * 1024 * 1024
         ),
     )(
         states, mix_gain[None, :], w_value, w_gate, conv_kernel, chan_gain[None, :], w_mix,

time: 174 us -> 168 us (0.966)
  Pallas kernels: 171 us -> 165 us
    pallas_call x1, Pallas kernels: 171 us -> 165 us  [plane_body(): pl.pallas_call(functools.partial(plane_kernel, (reps, n, tps, rows, chann...]
where the time goes in v3:
time: 168 us; the launch traced here: 166 us
  Pallas kernels  165 us (98%)
    pallas_call x1, Pallas kernels, plane_body(): pl.pallas_call(functools.partial(plane_kernel, (reps, n, tps, rows, chann...  165 us

profile of v3, /device:TPU:24, one launch (start us, length us, event | category | flops | bytes accessed | tf_op | source)
XLA Modules:
  0.0 166.3 jit_solution(6192811831704228885)
XLA Ops:
  0.0 165.4 %shard_map.100 = bf16[384,1024]{1,0:T(8,128)(2,1)S(1)} custom-call(bf16[384,1024]{1,0:T(8,128)(2,1)} %states.1, f32[1,2048]{1,0:T(1,128)} %bitcast.3, bf16[256,1024]{1,0:T(8,128)(2,1)} %w_value.1, bf16[256,1024]{1,0:T(8,128)(2,1)} %w_gate.1, f32[31,2048]{1,0:T(8,128)} %taps_in.1, f32[1,2048]{1,0:T(1,128)} %bitcast.4, bf16[256,1024]{1,0:T(8,128)(2,1)} %w_mix.1, ...), custom_call_target="tpu_custom_call" | custom-call | tf_op jit(solution)/shard_map/pallas_call | solution.py:1243
  165.4 0.9 copy.12

commit v4 on v3

--- a/solution.py
+++ b/solution.py
@@ -482,11 +482,12 @@
     out,
     mix_gain, conv_kernel, chan_gain, mlp_gain,
     weights, rows_in, rows_mid, normed, padded, filtered, activated, hidden, own_in, own_mid,
-    own_stats, peer_stats, mix_parts, stage, mix_peers, fed_parts, fed_peers,
+    own_stats, peer_stats, mix_parts, stage, mix_peers, fed_parts, fed_stage, fed_peers,
     load_sems, y_send, y_recv, near_send, far_send, line_recv, last_recv,
     twin_send, twin_recv, last_twin,
     in_send, in_recv, mid_send, mid_recv,
     stat_send, stat_recv, stage_send, stage_recv, mix_send, mix_recv, fed_send, fed_recv,
+    fed_stage_send, fed_stage_recv, fed_pass_send,
 ):
     reps, n, tps, rows, channels, sub, ups = sizes
     ys = tps
@@ -618,12 +619,15 @@
         at = weights.at[chunk, span, half]
         return remote(at, at, send, recv, **where)
 
+    def batch_of(c):
+        return 0 if c < 3 else 1 if c < 3 + ups else 2
+
     def group_of(c):
         return slice(0, 2) if c < 2 else c if c == 2 else slice(3, 3 + ups)
 
     def twin(c, i):
         return moved(
-            c, rows_of(planes[i], plane_shard), twin_send.at[c], twin_recv.at[0 if c < 2 else min(c - 1, 2)],
+            c, rows_of(planes[i], plane_shard), twin_send.at[batch_of(c)], twin_recv.at[0 if c < 2 else min(c - 1, 2)],
             tp=other_tp,
         )
 
@@ -634,7 +638,7 @@
 
     def twin_last(c, i, b, h):
         return moved(
-            c, half_rows(planes[i] * ys + b, h), twin_send.at[c], last_twin.at[i, b, h],
+            c, half_rows(planes[i] * ys + b, h), twin_send.at[batch_of(c)], last_twin.at[i, b, h],
             tp=other_tp,
         )
 
@@ -642,7 +646,7 @@
         group = group_of(c)
         whole_half = weights.at[group, :, half]
         remote(
-            whole_half, whole_half, twin_send.at[c], twin_recv.at[0 if c < 2 else min(c - 1, 2)], tp=other_tp
+            whole_half, whole_half, twin_send.at[batch_of(c)], twin_recv.at[0 if c < 2 else min(c - 1, 2)], tp=other_tp
         ).wait_recv()
 
     def ready_last(i, b, h):
@@ -716,8 +720,9 @@
             twin_last(c, i, b, h).start()
 
     @scoped("drain")
-    def drain(chunk):
-        moved(chunk, slice(None), twin_send.at[chunk], twin_recv.at[0], tp=other_tp).wait_send()
+    def drain(k):
+        batch = slice((0, 3, 3 + ups)[k], (3, 3 + ups, chunks)[k])
+        moved(batch, slice(None), twin_send.at[k], twin_recv.at[0], tp=other_tp).wait_send()
 
     @scoped("drain_all")
     def drain_all():
@@ -1008,27 +1013,115 @@
 
     @scoped("peers")
     def wait_peers(j, parts, peers, send, recv):
-        def some(start):
-            at = peers.at[start:, j]
+        def some(start, stop):
+            at = peers.at[start:stop, j]
             return remote(at, at, send.at[0], recv.at[j], rep=other_rep)
+
+        direct = (tp * per_tp + j) // ys == planes[zs - 1]
+        for is_direct, stop in ((direct, members), (jnp.logical_not(direct), 2)):
+            pl.when(jnp.logical_and(is_home, is_direct))(some(1, stop).wait_recv)
+            pl.when(jnp.logical_and(not_home, is_direct))(some(0, stop).wait_recv)
 
         @pl.when(is_home)
         def _():
             peers[0, j] = parts[tp * per_tp + j, rep_rows(rep), :]
-            some(1).wait_recv()
-
-        pl.when(not_home)(some(0).wait_recv)
+
+        return direct
+
+    def term_of(o, dr, part, k, c, left):
+        at = rep_rows(lax.rem(rep + dr, reps))
+        span = pl.ds(pl.multiple_of(o * block + part[0], part[1]), part[1])
+        return times_transposed(left[at, k * width : (k + 1) * width], weights[c, span, :])
+
+    def fed_stage_copy(i, b, r):
+        o, k = planes[i] * ys + b, i * ys + b
+        if b % 2 == 0:
+            return remote(
+                fed_parts.at[o, rep_rows(other_rep), :], fed_stage.at[k, 0],
+                fed_stage_send.at[0], fed_stage_recv.at[k], rep=other_rep,
+            )
+        return remote(
+            fed_parts.at[o, rep_rows(r), :], fed_stage.at[k, r],
+            fed_stage_send.at[1], fed_stage_recv.at[k], fs=z * ys + tp,
+        )
+
+    @scoped("fed_share")
+    def fed_share(i, b):
+        o = planes[i] * ys + b
+        for dr in (*range(1, reps), 0):
+            to = lax.rem(rep + dr, reps)
+            total = None
+            for k, c in enumerate(fourth):
+                term = term_of(o, dr, (0, block), k, c, hidden)
+                total = term if total is None else total + term
+            fed_parts[o, rep_rows(to), :] = total.astype(jnp.bfloat16)
+            if b % 2:
+                pl.when(not_home)(fed_stage_copy(i, b, to).start)
+            elif dr:
+                fed_stage_copy(i, b, to).start()
+
+    @scoped("fed_combine")
+    def fed_combine(i, b):
+        o, k = planes[i] * ys + b, i * ys + b
+        keeper, kept = o // per_tp, lax.rem(o, per_tp)
+        own_part = fed_parts.at[o, rep_rows(rep), :]
+        inside = remote(
+            own_part, fed_peers.at[0, kept], fed_pass_send.at[0], fed_recv.at[kept], tp=keeper
+        )
+
+        def add(r, slot):
+            at = rep_rows(r)
+            total = fed_parts[o, at, :].astype(jnp.float32) + fed_stage[k, slot].astype(
+                jnp.float32
+            )
+            fed_parts[o, at, :] = total.astype(jnp.bfloat16)
+
+        if b % 2 == 0:
+            fed_stage_copy(i, b, 0).wait_recv()
+            add(rep, 0)
+            outside = remote(
+                own_part, fed_peers.at[1, kept], fed_pass_send.at[1], fed_recv.at[kept],
+                fs=z * ys + tp, tp=keeper,
+            )
+            pl.when(not_home)(outside.start)
+            pl.when(jnp.logical_and(is_home, keeper != tp))(inside.start)
+        else:
+            outside = remote(
+                fed_parts.at[o, rep_rows(other_rep), :], fed_peers.at[1, kept],
+                fed_pass_send.at[1], fed_recv.at[kept], rep=other_rep, tp=keeper,
+            )
+
+            @pl.when(is_home)
+            def _():
+                both = fed_stage.at[k]
+                remote(
+                    both, both, fed_stage_send.at[1], fed_stage_recv.at[k], fs=other_fs
+                ).wait_recv()
+                for r in range(reps):
+                    add(r, r)
+                outside.start()
+                pl.when(keeper != tp)(inside.start)
 
     def settle_share(parts, send, recv):
-        for dr in range(reps):
-            for count, who in ((per_tp, is_home), (blocks, not_home)):
-                sent = parts.at[: count if dr == 0 else blocks, rep_rows(rep), :]
-                copy = remote(sent, sent, send.at[dr], recv.at[0], rep=other_rep)
-                pl.when(who)(copy.wait_send)
-
-    def total_of(j, peers):
+        def sent(count, sem):
+            at = parts.at[:count, rep_rows(rep), :]
+            return remote(at, at, sem, recv.at[0], rep=other_rep).wait_send
+
+        last_away = planes[zs - 1] * ys // per_tp != tp
+        last_here = jnp.logical_not(last_away)
+        for dr in range(1, reps):
+            sent(ys, send.at[dr])()
+        pl.when(jnp.logical_or(not_home, last_away))(sent(ys, send.at[0]))
+        sent(zs - 1, fed_stage_send.at[0])()
+        pl.when(not_home)(sent((zs - 1) * reps, fed_stage_send.at[1]))
+        sent(zs - 1, fed_pass_send.at[1])()
+        if per_tp > ys:
+            pl.when(jnp.logical_and(is_home, last_away))(sent(per_tp - ys, fed_pass_send.at[0]))
+        pl.when(jnp.logical_and(is_home, last_here))(sent(per_tp, fed_pass_send.at[0]))
+
+    def total_of(j, peers, count):
         total = peers[0, j].astype(jnp.float32)
-        for k in range(1, members):
+        for k in range(1, count):
             total = total + peers[k, j].astype(jnp.float32)
         return total
 
@@ -1070,17 +1163,18 @@
     own(1)
     across(2).start()
     across(3).start()
+    begin(2)
     padded[0:LEAD, :] = jnp.zeros((LEAD, width), jnp.float32)
     arrive(0, 1)
+    inner(pump(0, 2))
     arrive(1, 1)
+    inner(pump(1, 2))
     forward_in(0)
-    inner(pump(0, 2), pump(1, 2))
     for j in range(1, per_tp // 2):
         forward_in(j)
     inner(*[pump(c, i) for i in range(3, zs) for c in (0, 1)])
     for j in range(per_tp // 2, per_tp):
         forward_in(j)
-    begin(2)
     own(2)
     outer(*[pump(c, 2) for c in (0, 1)])
     for j in range(per_tp):
@@ -1094,10 +1188,10 @@
     outer(*[pump(c, i) for i in range(3, zs) for c in (0, 1)])
     ready(0)
 
-    inner(*all_of(2)[:1])
+    inner(*all_of(2)[:1], functools.partial(begin, 3))
     outer(*whole(3))
     inside = [
-        all_of(2)[1:2], all_of(2)[2:] + whole(3), whole(4), [],
+        all_of(2)[1:2], all_of(2)[2:] + [functools.partial(own, 3)], whole(4), [],
     ]
     outside = [whole(4), whole(5), whole(fourth[0]), sum([whole(c) for c in fourth[1:]], [])]
     for r in range(reps):
@@ -1124,13 +1218,13 @@
                 mix_share(t * per_tp + j, r)
 
     own_load.wait()
-    inner(*whole(5), *all_of(3)[:2])
+    inner(*whole(5), *all_of(3)[:2], *whole(fourth[0]))
     def last(i, b):
         return [functools.partial(arrive_last, i, b, h) for h in range(halves)]
 
     early = [
         all_of(3)[2:] + all_of(4)[:2],
-        all_of(4)[2:] + all_of(5)[:2] + whole(fourth[0]),
+        all_of(4)[2:] + all_of(5)[:2],
         all_of(5)[2:] + sum([whole(c) for c in fourth[1:]], []),
     ]
     late = [[], all_of(3), all_of(4)[:1], all_of(4)[1:]]
@@ -1166,6 +1260,7 @@
     for j in range(per_tp):
         finish_mid(j)
     outer(*all_of(5))
+    inner(*last(2, 0))
     norm_all(rows_mid, mlp_gain)
     ready(3)
 
@@ -1182,6 +1277,7 @@
 
     for k in range(ups):
         up_some(k)
+    pending = []
     fed = (hidden, fourth, fed_parts, fed_peers, fed_send, fed_recv)
     settle_in()
     settle_mid()
@@ -1190,35 +1286,45 @@
         stat_waits(r).wait_send()
     for i in range(zs):
         for b in range(ys):
-            if 1 < i + 1 < zs:
-                inner(*last(i + 1, b))
+            if i == 0 and b:
+                inner(*last(2, b))
+            if 0 < i < zs - 2:
+                inner(*last(i + 2, b))
             if i < zs - 1:
                 if i:
                     outer(*last(i, b))
                 for h in range(halves):
                     ready_last(i, b, h)
-                for dr in (*range(1, reps), 0):
-                    share(planes[i] * ys + b, dr, (0, block), *fed)
+                fed_share(i, b)
+                pending.append((i, b))
+                if len(pending) > 3:
+                    fed_combine(*pending.pop(0))
             else:
                 for h in range(halves):
                     outer(last(i, b)[h])
                     ready_last(i, b, h)
                     for dr in (*range(1, reps), 0):
                         share(planes[i] * ys + b, dr, (h * LANES, LANES), *fed)
+                    if pending:
+                        fed_combine(*pending.pop(0))
             if i == 1 and b == 0:
-                for c in range(3 + ups):
-                    drain(c)
+                drain(0)
+                drain(1)
+    while pending:
+        fed_combine(*pending.pop(0))
     for j in range(per_tp):
         if j == per_tp - 1:
-            for c in fourth:
-                drain(c)
+            drain(2)
             drain_all()
-        wait_peers(j, fed_parts, fed_peers, fed_send, fed_recv)
+        direct = wait_peers(j, fed_parts, fed_peers, fed_send, fed_recv)
         cols = slice(j * block, (j + 1) * block)
         with jax.named_scope("out"):
-            out[:, cols] = (
-                own_mid[:, cols].astype(jnp.float32) + total_of(j, fed_peers)
-            ).astype(jnp.bfloat16)
+            for is_direct, count in ((direct, members), (jnp.logical_not(direct), 2)):
+                @pl.when(is_direct)
+                def _():
+                    out[:, cols] = (
+                        own_mid[:, cols].astype(jnp.float32) + total_of(j, fed_peers, count)
+                    ).astype(jnp.bfloat16)
     with jax.named_scope("done"):
         settle_share(fed_parts, fed_send, fed_recv)
 
@@ -1266,6 +1372,7 @@
             pltpu.VMEM((blocks, reps, rows, block), bf16),
             pltpu.VMEM((2, per_tp, rows, block), bf16),
             pltpu.VMEM((blocks, tokens, block), bf16),
+            pltpu.VMEM(((zs - 1) * ys, reps, rows, block), bf16),
             pltpu.VMEM((members, per_tp, rows, block), bf16),
             dma((10,)),
             dma((1,)),
@@ -1274,7 +1381,7 @@
             dma((zs - 1,)),
             dma((3 + ups, zs)),
             dma((zs, ys, halves)),
-            dma((chunks,)),
+            dma((3,)),
             dma((3,)),
             dma((zs, ys, halves)),
             dma((5,)),
@@ -1289,6 +1396,9 @@
             dma((per_tp,)),
             dma((reps,)),
             dma((per_tp,)),
+            dma((2,)),
+            dma(((zs - 1) * ys,)),
+            dma((2,)),
         ],
         compiler_params=pltpu.CompilerParams(
             collective_id=0, has_side_effects=True, vmem_limit_bytes=56 * 1024 * 1024
@@ -1309,7 +1419,7 @@
         and n // tps > 2
         and own_width % (reps * tps * LANES) == 0
         and channels % (n * LANES) == 0
-        and own_width % (channels // n) == 0
+        and own_width % (tps * (channels // n)) == 0
     )
     return (plane_body if planar else ring_body)(mesh, states, *weights)
 

time: 168 us -> 167 us (level)
  no operation moved by 1% of the time
where the time goes in v4:
time: 167 us; the launch traced here: 165 us
  Pallas kernels  164 us (98%)
    pallas_call x1, Pallas kernels, plane_body(): pl.pallas_call(functools.partial(plane_kernel, (reps, n, tps, rows, chann...  164 us

profile of v4, /device:TPU:24, one launch (start us, length us, event | category | flops | bytes accessed | tf_op | source)
XLA Modules:
  0.0 165.0 jit_solution(3769095244766383335)
XLA Ops:
  0.0 164.1 %shard_map.100 = bf16[384,1024]{1,0:T(8,128)(2,1)S(1)} custom-call(bf16[384,1024]{1,0:T(8,128)(2,1)} %states.1, f32[1,2048]{1,0:T(1,128)} %bitcast.3, bf16[256,1024]{1,0:T(8,128)(2,1)} %w_value.1, bf16[256,1024]{1,0:T(8,128)(2,1)} %w_gate.1, f32[31,2048]{1,0:T(8,128)} %taps_in.1, f32[1,2048]{1,0:T(1,128)} %bitcast.4, bf16[256,1024]{1,0:T(8,128)(2,1)} %w_mix.1, ...), custom_call_target="tpu_custom_call" | custom-call | tf_op jit(solution)/shard_map/pallas_call | solution.py:1349
  164.1 0.9 copy.12

commit v5 on v4

--- a/solution.py
+++ b/solution.py
@@ -633,13 +633,23 @@
 
     halves = shard // LANES
 
+    def is_last(b, h):
+        return b == ys - 1 and h == halves - 1
+
+    def slot_of(c, part, h):
+        slot = part * halves + h
+        extra = c - fourth[0]
+        if isinstance(part, int):
+            return slot + extra if is_last(part, h) else slot
+        return slot + jnp.where(part == ys - 1, extra, 0) if h == halves - 1 else slot
+
     def half_rows(index, h):
         return rows_of(index * halves + h, LANES)
 
     def twin_last(c, i, b, h):
         return moved(
-            c, half_rows(planes[i] * ys + b, h), twin_send.at[batch_of(c)], last_twin.at[i, b, h],
-            tp=other_tp,
+            c, half_rows(planes[i] * ys + b, h), twin_send.at[batch_of(c)],
+            last_twin.at[i, slot_of(c, b, h)], tp=other_tp,
         )
 
     def ready(c):
@@ -649,11 +659,18 @@
             whole_half, whole_half, twin_send.at[batch_of(c)], twin_recv.at[0 if c < 2 else min(c - 1, 2)], tp=other_tp
         ).wait_recv()
 
-    def ready_last(i, b, h):
-        moved(
-            slice(3 + ups, chunks), half_rows(planes[i] * ys + b, h), twin_send.at[0],
-            last_twin.at[i, b, h], tp=other_tp,
-        ).wait_recv()
+    def ready_last(i, b, h, some=None):
+        def wait(chunk, first):
+            moved(
+                chunk, half_rows(planes[i] * ys + b, h), twin_send.at[0],
+                last_twin.at[i, slot_of(first, b, h)], tp=other_tp,
+            ).wait_recv()
+
+        if is_last(b, h):
+            for c in fourth if some is None else some:
+                wait(c, c)
+        else:
+            wait(slice(3 + ups, chunks), fourth[0])
 
     def near(c, way, part):
         if c not in fourth:
@@ -665,7 +682,8 @@
             ]
         return [
             moved(
-                c, half_rows(z * ys + part, h), near_send.at[way], last_recv.at[z, part, h],
+                c, half_rows(z * ys + part, h), near_send.at[way],
+                last_recv.at[z, slot_of(c, part, h)],
                 fs=next_fs[way],
             )
             for h in range(halves)
@@ -710,13 +728,18 @@
         twin(c, i).start()
 
     @scoped("arrive_last")
-    def arrive_last(i, b, h):
-        span, recv = half_rows(planes[i] * ys + b, h), last_recv.at[planes[i], b, h]
-        copy = onward(slice(3 + ups, chunks), i, span, recv)
-        copy.wait_recv()
-        for c in fourth:
-            pl.when(goes[i])(onward(c, i, span, recv).start)
-        for c in fourth:
+    def arrive_last(i, b, h, some=fourth):
+        span = half_rows(planes[i] * ys + b, h)
+
+        def copy(chunk, first):
+            return onward(chunk, i, span, last_recv.at[planes[i], slot_of(first, b, h)])
+
+        if not is_last(b, h):
+            copy(slice(3 + ups, chunks), fourth[0]).wait_recv()
+        for c in some:
+            if is_last(b, h):
+                copy(c, c).wait_recv()
+            pl.when(goes[i])(copy(c, c).start)
             twin_last(c, i, b, h).start()
 
     @scoped("drain")
@@ -897,18 +920,15 @@
         activated[seq_rows(i), :] = (x / (1.0 + jnp.exp(-x))).astype(jnp.bfloat16)
         return carry
 
-    @scoped("share")
-    def share(o, dr, part, left, pieces_of, parts, peers, send, recv):
+    def term_of(o, dr, part, k, c, left):
+        at = rep_rows(lax.rem(rep + dr, reps))
+        span = pl.ds(pl.multiple_of(o * block + part[0], part[1]), part[1])
+        return times_transposed(left[at, k * width : (k + 1) * width], weights[c, span, :])
+
+    def send_share(o, dr, part, total, parts, peers, send, recv):
         to = lax.rem(rep + dr, reps)
-        first, size = part
-        span = pl.ds(pl.multiple_of(o * block + first, size), size)
-        cols = pl.ds(first, size)
+        cols, at = pl.ds(*part), rep_rows(to)
         keeper, kept = o // per_tp, lax.rem(o, per_tp)
-        at = rep_rows(to)
-        total = None
-        for k, c in enumerate(pieces_of):
-            term = times_transposed(left[at, k * width : (k + 1) * width], weights[c, span, :])
-            total = term if total is None else total + term
         parts[o, at, cols] = total.astype(jnp.bfloat16)
         slot = lax.rem(rep + reps - to, reps) * ys + lax.rem(y + ys - tp, ys)
         copy = remote(
@@ -917,6 +937,14 @@
         )
         here = jnp.logical_and(is_home, jnp.logical_and(keeper == tp, to == rep))
         pl.when(jnp.logical_not(here))(copy.start)
+
+    @scoped("share")
+    def share(o, dr, part, left, pieces_of, *where):
+        total = None
+        for k, c in enumerate(pieces_of):
+            term = term_of(o, dr, part, k, c, left)
+            total = term if total is None else total + term
+        send_share(o, dr, part, total, *where)
 
     def along_first(o):
         return o % 2 == 0
@@ -1027,11 +1055,6 @@
             peers[0, j] = parts[tp * per_tp + j, rep_rows(rep), :]
 
         return direct
-
-    def term_of(o, dr, part, k, c, left):
-        at = rep_rows(lax.rem(rep + dr, reps))
-        span = pl.ds(pl.multiple_of(o * block + part[0], part[1]), part[1])
-        return times_transposed(left[at, k * width : (k + 1) * width], weights[c, span, :])
 
     def fed_stage_copy(i, b, r):
         o, k = planes[i] * ys + b, i * ys + b
@@ -1300,13 +1323,32 @@
                 if len(pending) > 3:
                     fed_combine(*pending.pop(0))
             else:
+                o, ways = planes[i] * ys + b, (*range(1, reps), 0)
+                final = functools.partial(arrive_last, i, b, halves - 1)
                 for h in range(halves):
-                    outer(last(i, b)[h])
-                    ready_last(i, b, h)
-                    for dr in (*range(1, reps), 0):
-                        share(planes[i] * ys + b, dr, (h * LANES, LANES), *fed)
-                    if pending:
-                        fed_combine(*pending.pop(0))
+                    part = (h * LANES, LANES)
+                    if not is_last(b, h):
+                        outer(last(i, b)[h])
+                        ready_last(i, b, h)
+                        for n_way, dr in enumerate(ways):
+                            share(o, dr, part, *fed)
+                            if n_way == 0 and is_last(b, h + 1):
+                                outer(functools.partial(final, fourth[:-1]))
+                        for _ in range(2):
+                            if pending:
+                                fed_combine(*pending.pop(0))
+                        continue
+                    if halves == 1:
+                        outer(functools.partial(final, fourth[:-1]))
+                    outer(functools.partial(final, fourth[-1:]))
+                    totals = [None] * reps
+                    for k, c in enumerate(fourth):
+                        ready_last(i, b, h, (c,))
+                        for dr in ways:
+                            term = term_of(o, dr, part, k, c, hidden)
+                            totals[dr] = term if k == 0 else totals[dr] + term
+                            if k == ups - 1:
+                                send_share(o, dr, part, totals[dr], *fed[2:])
             if i == 1 and b == 0:
                 drain(0)
                 drain(1)
@@ -1380,10 +1422,10 @@
             dma((2,)),
             dma((zs - 1,)),
             dma((3 + ups, zs)),
-            dma((zs, ys, halves)),
+            dma((zs, ys * halves + ups - 1)),
             dma((3,)),
             dma((3,)),
-            dma((zs, ys, halves)),
+            dma((zs, ys * halves + ups - 1)),
             dma((5,)),
             dma((reps, tps, per_tp)),
             dma((5,)),

time: 167 us -> 166 us (level)
  no operation moved by 1% of the time
where the time goes in v5:
time: 166 us; the launch traced here: 164 us
  Pallas kernels  163 us (98%)
    pallas_call x1, Pallas kernels, plane_body(): pl.pallas_call(functools.partial(plane_kernel, (reps, n, tps, rows, chann...  163 us

profile of v5, /device:TPU:24, one launch (start us, length us, event | category | flops | bytes accessed | tf_op | source)
XLA Modules:
  0.0 164.1 jit_solution(17984326904516001380)
XLA Ops:
  0.0 163.2 %shard_map.100 = bf16[384,1024]{1,0:T(8,128)(2,1)S(1)} custom-call(bf16[384,1024]{1,0:T(8,128)(2,1)} %states.1, f32[1,2048]{1,0:T(1,128)} %bitcast.3, bf16[256,1024]{1,0:T(8,128)(2,1)} %w_value.1, bf16[256,1024]{1,0:T(8,128)(2,1)} %w_gate.1, f32[31,2048]{1,0:T(8,128)} %taps_in.1, f32[1,2048]{1,0:T(1,128)} %bitcast.4, bf16[256,1024]{1,0:T(8,128)(2,1)} %w_mix.1, ...), custom_call_target="tpu_custom_call" | custom-call | tf_op jit(solution)/shard_map/pallas_call | solution.py:1391
  163.2 0.9 copy.12
